TPU v7x, 32 devices: a whole 2x2x4 slice. The times are simulated.
32 devices in a mesh: sp: 8 (over z, x), tp: 4 (over y, core).
Axes of the slice: x: 2, y: 2, z: 4, core: 2. Of those that a mesh axis runs over, the one named last changes fastest.
Arguments:
- moe_input: bfloat16 [1024, 2048], P('sp'), may hold values from -6 to 6
- out_grad: bfloat16 [1024, 2048], P('sp'), may hold values from -6 to 6
- routes: int32 [1024, 2], P('sp'), may hold values from 0 to 3, all different within a row; in each aligned block of 128 rows (0 to 127, 128 to 255, ...) at most 96 rows name the same one
- route_weights: float32 [1024, 2], P('sp'), may hold values from 0.2 to 1
- gate_cols: bfloat16 [2048, 14336], P(None, ('sp', 'tp')), may hold values from -0.125 to 0.125
- up_cols: bfloat16 [2048, 14336], P(None, ('sp', 'tp')), may hold values from -0.125 to 0.125
- down_rows: bfloat16 [14336, 2048], P(('sp', 'tp')), may hold values from -0.09375 to 0.09375
- out_proj: bfloat16 [2048, 512], P(None, 'tp'), may hold values from -0.25 to 0.25
- conv_out: bfloat16 [1024, 512], P('sp', 'tp'), may hold values from -6 to 6
- gate_b: bfloat16 [1024, 512], P('sp', 'tp'), may hold values from -6 to 6
- gate_c: bfloat16 [1024, 512], P('sp', 'tp'), may hold values from -6 to 6
- hidden_h: bfloat16 [1024, 512], P('sp', 'tp'), may hold values from -6 to 6
- conv_taps: float32 [3, 512], P(None, 'tp'), may hold values from -3.5 to 3.5
Outputs:
- grad_gate: bfloat16 [2048, 14336], P(None, ('sp', 'tp'))
- grad_up: bfloat16 [2048, 14336], P(None, ('sp', 'tp'))
- grad_down: bfloat16 [14336, 2048], P(('sp', 'tp'))
- grad_proj: float32 [2048, 512], P('sp', 'tp')
- grad_hidden: bfloat16 [1024, 512], P('sp', 'tp')
- grad_gate_b: bfloat16 [1024, 512], P('sp', 'tp')
- grad_gate_c: bfloat16 [1024, 512], P('sp', 'tp')
Inputs may be any that keep to these rules, and one draw needn't show every extreme that they name: `routes`: each row names 2 different experts. Among the rows of one device no expert is named more than 96 times, a bound that some block reaches.
All inputs are finite; a program needn't handle non-finite values.
Results may differ from a plain program's by a relative error of at most 0.01.
Values may be sent and summed in bfloat16 or wider, within the bound.
A program may use at most 128 MiB of HBM per device.

v0:
```python
import functools

import jax
import jax.numpy as jnp
from jax import lax
from jax.experimental import pallas as pl
from jax.experimental.pallas import tpu as pltpu
from jax.sharding import PartitionSpec as P


def from_behind(block, axis, distance):
    devices = range(lax.axis_size(axis))
    route = [(i - distance, i) for i in devices if i - distance in devices]
    return lax.ppermute(block, axis, route)


MESH = pl.DeviceIdType.MESH
VMEM = pl.BlockSpec(memory_space=pltpu.VMEM)


def columns(index, width):
    return pl.ds(pl.multiple_of(index * width, width), width)


def wait_arrival(ref, sem):
    pltpu.make_async_copy(ref, ref, sem).wait()


def greet(peers):
    barrier = pltpu.get_barrier_semaphore()
    for peer in peers:
        pl.semaphore_signal(barrier, inc=1, device_id=peer, device_id_type=MESH)
    pl.semaphore_wait(barrier, len(peers))


def place(n_tp):
    sp, tp = lax.axis_index("sp"), lax.axis_index("tp")
    expert, parity = sp // 2, lax.rem(sp, 2)
    row, core = tp // 2, lax.rem(tp, 2)
    return sp, tp, expert, parity, row, core


def dispatch_kernel(
    n_sp, n_tp, chunks,
    x_ref, g_ref, branch_ref, head_ref,
    out_x, out_g, out_b, out_head,
    z_send, z_recv, own_send, relay_send, near_recv, diag_recv, pair_send, pair_recv, b_send, b_recv, h_send, h_recv,
):
    experts = n_sp // 2
    sp, tp, expert, parity, row, core = place(n_tp)
    width = x_ref.shape[-1]
    size = experts // chunks
    x_side = (2 * expert + 1 - parity, tp)
    y_side = (sp, 2 * (1 - row) + core)
    pair = (sp, 2 * row + 1 - core)
    greet([(lax.rem(sp + d, n_sp), tp) for d in range(1, n_sp)] + [y_side, pair])
    started = []
    sources, outs = (x_ref, g_ref), (out_x, out_g)

    def spot(t, par, first, quarter, count):
        return outs[t].at[par, pl.ds(first, count), :, columns(quarter, width)]

    def send(src, device, send_sem, recv_sem):
        copy = pltpu.make_async_remote_copy(
            src_ref=src, dst_ref=src, send_sem=send_sem, recv_sem=recv_sem,
            device_id=device, device_id_type=MESH,
        )
        copy.start()
        started.append(copy)

    for t in range(2):
        for d in range(experts):
            target = lax.rem(expert + d, experts)
            src = sources[t].at[pl.ds(target, 1)]
            dst = spot(t, parity, expert, tp, 1)
            if d == 0:
                pltpu.make_async_copy(src, dst, z_recv.at[t, 0]).start()
                continue
            copy = pltpu.make_async_remote_copy(
                src_ref=src, dst_ref=dst, send_sem=z_send.at[t, d], recv_sem=z_recv.at[t, d],
                device_id=(2 * target + parity, tp), device_id_type=MESH,
            )
            copy.start()
            started.append(copy)
    for d in range(n_sp):
        dst = out_b.at[sp]
        if d == 0:
            pltpu.make_async_copy(branch_ref, dst, b_recv.at[0]).start()
            continue
        copy = pltpu.make_async_remote_copy(
            src_ref=branch_ref, dst_ref=dst, send_sem=b_send.at[d], recv_sem=b_recv.at[d],
            device_id=(lax.rem(sp + d, n_sp), tp), device_id_type=MESH,
        )
        copy.start()
        started.append(copy)

    copy = pltpu.make_async_remote_copy(
        src_ref=head_ref, dst_ref=out_head, send_sem=h_send.at[0], recv_sem=h_recv.at[0],
        device_id=(lax.rem(sp + n_sp - 1, n_sp), tp), device_id_type=MESH,
    )
    copy.start()
    started.append(copy)

    own_chunk = expert // size
    other_quarter = 2 * (1 - row) + core

    def first_of(k):
        return lax.rem(own_chunk + chunks - k, chunks) * size

    def own_stage(k, t):
        first = first_of(k)
        for i in range(size):
            source = first + i
            d = lax.rem(expert + experts - source, experts)
            wait_arrival(spot(t, parity, source, tp, 1), z_recv.at[t, d])
        block = spot(t, parity, first, tp, size)
        send(block, x_side, own_send.at[t, k, 0], near_recv.at[t, k, 0])
        send(block, y_side, own_send.at[t, k, 1], near_recv.at[t, k, 1])
        send(block, pair, pair_send.at[t, k, 0], pair_recv.at[t, k, 0])

    def near_stage(k, t):
        first = first_of(k)
        from_x = spot(t, 1 - parity, first, tp, size)
        from_y = spot(t, parity, first, other_quarter, size)
        wait_arrival(from_x, near_recv.at[t, k, 0])
        if (k + t) % 2 == 0:
            send(from_x, y_side, relay_send.at[t, k], diag_recv.at[t, k])
        send(from_x, pair, pair_send.at[t, k, 1], pair_recv.at[t, k, 1])
        wait_arrival(from_y, near_recv.at[t, k, 1])
        if (k + t) % 2 == 1:
            send(from_y, x_side, relay_send.at[t, k], diag_recv.at[t, k])
        send(from_y, pair, pair_send.at[t, k, 2], pair_recv.at[t, k, 2])

    def far_stage(k, t):
        block = spot(t, 1 - parity, first_of(k), other_quarter, size)
        wait_arrival(block, diag_recv.at[t, k])
        send(block, pair, pair_send.at[t, k, 3], pair_recv.at[t, k, 3])

    order = [0] + [k for n in range(1, chunks // 2 + 1) for k in dict.fromkeys((n, chunks - n))]
    steps = [(k, t) for k in order for t in range(2)]
    for n in range(len(steps) + 3):
        if n < len(steps):
            own_stage(*steps[n])
        if 1 <= n < len(steps) + 1:
            near_stage(*steps[n - 1])
        if 3 <= n < len(steps) + 3:
            far_stage(*steps[n - 3])
    for k, t in steps:
        first = first_of(k)
        quarters = (2 * row + 1 - core, 2 * (1 - row) + 1 - core)
        spots = ((parity, quarters[0]), (1 - parity, quarters[0]),
                 (parity, quarters[1]), (1 - parity, quarters[1]))
        for j, (par, quarter) in enumerate(spots):
            wait_arrival(spot(t, par, first, quarter, size), pair_recv.at[t, k, j])
    for d in range(n_sp):
        wait_arrival(out_b.at[lax.rem(sp + n_sp - d, n_sp)], b_recv.at[d])
    wait_arrival(out_head, h_recv.at[0])
    for copy in started:
        copy.wait_send()


def dispatch(x, g, branch, head, n_sp, n_tp):
    experts, capacity, width = x.shape
    chunks = min(experts, 4)
    dma = pltpu.SemaphoreType.DMA
    rows = jax.ShapeDtypeStruct((2, experts, capacity, width * n_tp), jnp.bfloat16)
    return pl.pallas_call(
        functools.partial(dispatch_kernel, n_sp, n_tp, chunks),
        out_shape=(
            rows, rows, jax.ShapeDtypeStruct((n_sp,) + branch.shape, branch.dtype),
            jax.ShapeDtypeStruct(head.shape, head.dtype),
        ),
        in_specs=[VMEM] * 4,
        out_specs=(VMEM,) * 4,
        scratch_shapes=[
            dma((2, experts)), dma((2, experts)), dma((2, chunks, 2)), dma((2, chunks)),
            dma((2, chunks, 2)), dma((2, chunks)), dma((2, chunks, 4)), dma((2, chunks, 4)),
            dma((n_sp,)), dma((n_sp,)), dma((1,)), dma((1,)),
        ],
        compiler_params=pltpu.CompilerParams(
            collective_id=0, has_side_effects=True, vmem_limit_bytes=48 * 1024 * 1024
        ),
    )(x, g, branch, head)


def return_kernel(
    n_sp, n_tp, chunks,
    part_ref, out_ref,
    from_pair, summed, from_chips, final,
    pair_send, pair_recv, chip_send, chip_recv, z_send, z_recv,
):
    experts = n_sp // 2
    sp, tp, expert, parity, row, core = place(n_tp)
    width = out_ref.shape[-1]
    pair = (sp, 2 * row + 1 - core)
    offsets = ((1, 1), (1, 0), (0, 1), (0, 0))

    def other(dp, dr):
        return lax.rem(parity + dp, 2), lax.rem(row + dr, 2)

    chips = [(2 * expert + other(dp, dr)[0], 2 * other(dp, dr)[1] + core) for dp, dr in offsets[:3]]
    along = [(2 * lax.rem(expert + d, experts) + parity, tp) for d in range(1, experts)]
    greet([pair] + chips + along)
    started, guarded = [], []

    def send(src, dst, send_sem, recv_sem, device):
        copy = pltpu.make_async_remote_copy(
            src_ref=src, dst_ref=dst, send_sem=send_sem, recv_sem=recv_sem,
            device_id=device, device_id_type=MESH,
        )
        copy.start()
        started.append(copy)

    size = experts // chunks
    own_chunk = expert // size
    order = [chunks // 2] if chunks > 1 else []
    order += [k for k in range(1, chunks) if k not in order] + [0]

    def first_of(k):
        return lax.rem(own_chunk + k, chunks) * size

    for k in order:
        part = pl.ds(first_of(k), size)
        for n, (dp, dr) in enumerate(offsets):
            par, line = other(dp, dr)
            src = part_ref.at[par, part, :, columns(2 * line + 1 - core, width)]
            send(src, from_pair.at[n, part], pair_send.at[n, k], pair_recv.at[n, k], pair)
    for k in order:
        first = first_of(k)
        part = pl.ds(first, size)
        for n, (dp, dr) in enumerate(offsets):
            par, line = other(dp, dr)
            wait_arrival(from_pair.at[n, part], pair_recv.at[n, k])
            for i in range(size):
                mine = part_ref[par, first + i, :, columns(2 * line + core, width)]
                total = mine.astype(jnp.float32) + from_pair[n, first + i].astype(jnp.float32)
                summed[n, first + i] = total.astype(jnp.bfloat16)
            if n < 3:
                send(summed.at[n, part], from_chips.at[n, part], chip_send.at[n, k],
                     chip_recv.at[n, k], chips[n])
    for k in order:
        first = first_of(k)
        part = pl.ds(first, size)
        for n in range(3):
            wait_arrival(from_chips.at[n, part], chip_recv.at[n, k])
        for i in range(size):
            target = first + i
            total = summed[3, target].astype(jnp.float32)
            for n in range(3):
                total = total + from_chips[n, target].astype(jnp.float32)
            final[target] = total.astype(jnp.bfloat16)
            away = target != expert
            copy = pltpu.make_async_remote_copy(
                src_ref=final.at[target], dst_ref=out_ref.at[expert],
                send_sem=z_send.at[target], recv_sem=z_recv.at[expert],
                device_id=(2 * target + parity, tp), device_id_type=MESH,
            )
            if size == 1 and k:
                copy.start()
                started.append(copy)
                continue
            if size == 1:
                out_ref[expert] = final[target]
                continue

            @pl.when(away)
            def _(copy=copy):
                copy.start()

            @pl.when(jnp.logical_not(away))
            def _():
                out_ref[expert] = final[expert]

            guarded.append((away, copy))
    for d in range(1, experts):
        source = lax.rem(expert + experts - d, experts)
        wait_arrival(out_ref.at[source], z_recv.at[source])
    for copy in started:
        copy.wait_send()
    for away, copy in guarded:
        pl.when(away)(copy.wait_send)


def give_back(part, n_sp, n_tp):
    _, experts, capacity, model_width = part.shape
    width = model_width // n_tp
    dma = pltpu.SemaphoreType.DMA
    block = (experts, capacity, width)
    chunks = min(experts, 4)
    return pl.pallas_call(
        functools.partial(return_kernel, n_sp, n_tp, chunks),
        out_shape=jax.ShapeDtypeStruct(block, jnp.bfloat16),
        in_specs=[VMEM],
        out_specs=VMEM,
        scratch_shapes=[
            pltpu.VMEM((4,) + block, jnp.bfloat16), pltpu.VMEM((4,) + block, jnp.bfloat16),
            pltpu.VMEM((3,) + block, jnp.bfloat16), pltpu.VMEM(block, jnp.bfloat16),
            dma((4, chunks)), dma((4, chunks)), dma((3, chunks)), dma((3, chunks)),
            dma((experts,)), dma((experts,)),
        ],
        compiler_params=pltpu.CompilerParams(
            collective_id=1, has_side_effects=True, vmem_limit_bytes=48 * 1024 * 1024
        ),
    )(part)


def stream_kernel(
    n_sp, n_tp, part_ref, stream_ref, block_ref,
    tp_send, tp_recv, h_send, h_recv, b_send, b_recv, s_send, s_recv,
):
    sp, tp = lax.axis_index("sp"), lax.axis_index("tp")
    tokens, width = part_ref.shape
    block = block_ref.shape[2]
    halo = stream_ref.shape[0] - tokens
    per_part, per_peer = width // block, n_sp // n_tp
    greet([
        (lax.rem(sp + i, n_sp), lax.rem(tp + j, n_tp))
        for i in range(n_sp) for j in range(n_tp) if i or j
    ])
    started = []

    def send(src, dst, send_sem, recv_sem, device):
        copy = pltpu.make_async_remote_copy(
            src_ref=src, dst_ref=dst, send_sem=send_sem, recv_sem=recv_sem,
            device_id=device, device_id_type=MESH,
        )
        copy.start()
        started.append((None, copy))

    keeper = sp // per_peer
    for b in range(per_part):
        target = tp * per_part + b
        src = part_ref.at[:, b * block : (b + 1) * block]
        dst = block_ref.at[sp]
        away = jnp.logical_or(target != sp, keeper != tp)
        copy = pltpu.make_async_remote_copy(
            src_ref=src, dst_ref=dst, send_sem=b_send.at[b], recv_sem=b_recv.at[lax.rem(sp, per_peer)],
            device_id=(target, keeper), device_id_type=MESH,
        )

        @pl.when(away)
        def _(copy=copy):
            copy.start()

        @pl.when(jnp.logical_not(away))
        def _(src=src, dst=dst):
            pltpu.make_async_copy(src, dst, b_recv.at[lax.rem(sp, per_peer)]).start()

        started.append((away, copy))
    mine = stream_ref.at[pl.ds(0, tokens), columns(tp, width)]
    edge = stream_ref.at[pl.ds(tokens, halo), columns(tp, width)]
    before = lax.rem(sp + n_sp - 1, n_sp)
    pltpu.make_async_copy(part_ref, mine, tp_recv.at[0]).start()
    for j in range(n_tp):
        peer = lax.rem(tp + j, n_tp)
        if j:
            send(part_ref, mine, tp_send.at[j], tp_recv.at[j], (sp, peer))
        send(part_ref.at[pl.ds(0, halo)], edge, h_send.at[j], h_recv.at[j], (before, peer))
    for n in range(per_peer):
        held = block_ref.at[tp * per_peer + n]
        wait_arrival(held, b_recv.at[n])
        for j in range(1, n_tp):
            send(held, held, s_send.at[n, j], s_recv.at[n, j], (sp, lax.rem(tp + j, n_tp)))
    for j in range(n_tp):
        source = lax.rem(tp + n_tp - j, n_tp)
        wait_arrival(stream_ref.at[pl.ds(0, tokens), columns(source, width)], tp_recv.at[j])
        wait_arrival(stream_ref.at[pl.ds(tokens, halo), columns(source, width)], h_recv.at[j])
        for n in range(per_peer):
            if j:
                wait_arrival(block_ref.at[source * per_peer + n], s_recv.at[n, j])
    for away, copy in started:
        if away is None:
            copy.wait_send()
        else:
            pl.when(away)(copy.wait_send)


def share_stream(part, halo, n_sp, n_tp):
    tokens, width = part.shape
    dma = pltpu.SemaphoreType.DMA
    block = width * n_tp // n_sp
    per_peer = n_sp // n_tp
    return pl.pallas_call(
        functools.partial(stream_kernel, n_sp, n_tp),
        out_shape=(
            jax.ShapeDtypeStruct((tokens + halo, width * n_tp), jnp.bfloat16),
            jax.ShapeDtypeStruct((n_sp, tokens, block), jnp.bfloat16),
        ),
        in_specs=[VMEM],
        out_specs=(VMEM, VMEM),
        scratch_shapes=[
            dma((n_tp,)), dma((n_tp,)), dma((n_tp,)), dma((n_tp,)),
            dma((width // block,)), dma((per_peer,)), dma((per_peer, n_tp)), dma((per_peer, n_tp)),
        ],
        compiler_params=pltpu.CompilerParams(collective_id=2, has_side_effects=True),
    )(part)


def slot_choice(routes, experts, capacity):
    flat_ids = routes.reshape(-1)
    one_hot = (flat_ids[:, None] == jnp.arange(experts, dtype=jnp.int32)[None, :])
    count = flat_ids.shape[0]
    before = jnp.arange(count)[:, None] > jnp.arange(count)[None, :]
    earlier = jnp.dot(
        before.astype(jnp.bfloat16), one_hot.astype(jnp.bfloat16), preferred_element_type=jnp.float32
    )
    ranked = jnp.sum(jnp.where(one_hot, earlier, 0.0), axis=1).astype(jnp.int32)
    return (flat_ids * capacity + ranked).reshape(routes.shape)


def contract_rows(left_side, right_side):
    return lax.dot_general(
        left_side, right_side, (((0,), (0,)), ((), ())), preferred_element_type=jnp.float32
    )


def contract_cols(left_side, right_side):
    return lax.dot_general(
        left_side, right_side, (((1,), (1,)), ((), ())), preferred_element_type=jnp.float32
    )


def per_device(
    moe_input,
    out_grad,
    routes,
    route_weights,
    gate_cols,
    up_cols,
    down_rows,
    out_proj,
    conv_out,
    gate_b,
    gate_c,
    hidden_h,
    conv_taps,
):
    seq_devices = lax.axis_size("sp")
    experts = seq_devices // 2
    tokens_here, model_width = moe_input.shape
    top_count = routes.shape[1]
    half_cap = 3 * tokens_here // seq_devices
    capacity = 2 * half_cap
    slot_count = experts * capacity
    n_tp = lax.axis_size("tp")
    positions = slot_choice(routes, experts, capacity)
    slots = jnp.arange(slot_count, dtype=jnp.int32)
    hits = slots[:, None, None] == positions[None]
    chosen = jnp.any(hits, axis=2).astype(jnp.bfloat16)
    slot_weight = jnp.sum(jnp.where(hits, route_weights[None], 0.0), axis=(1, 2))
    quarter = model_width // n_tp
    column_start = lax.axis_index("tp") * quarter
    source_x = lax.dynamic_slice_in_dim(moe_input, column_start, quarter, 1)
    source_g = lax.dynamic_slice_in_dim(out_grad, column_start, quarter, 1)
    sent_x = jnp.dot(chosen, source_x, preferred_element_type=jnp.float32).astype(jnp.bfloat16)
    sent_g = jnp.dot(chosen, source_g, preferred_element_type=jnp.float32)
    sent_g = (slot_weight[:, None] * sent_g).astype(jnp.bfloat16)
    branch = (gate_b.astype(jnp.float32) * conv_out.astype(jnp.float32)).astype(jnp.bfloat16)
    halo = 16
    rows_x, rows_g, all_branch, next_gate_b = dispatch(
        sent_x.reshape(experts, capacity, quarter),
        sent_g.reshape(experts, capacity, quarter),
        branch,
        gate_b[:halo],
        seq_devices,
        n_tp,
    )
    rows_x = rows_x.reshape(-1, model_width)
    rows_g = rows_g.reshape(-1, model_width)
    gate_pre = jnp.dot(rows_x, gate_cols, preferred_element_type=jnp.float32)
    up_pre = jnp.dot(rows_x, up_cols, preferred_element_type=jnp.float32)
    sigmoid_g = jax.nn.sigmoid(gate_pre)
    silu_g = gate_pre * sigmoid_g
    activation = (silu_g * up_pre).astype(jnp.bfloat16)
    grad_down = contract_rows(activation, rows_g).astype(jnp.bfloat16)
    d_act = contract_cols(rows_g, down_rows)
    d_up = (d_act * silu_g).astype(jnp.bfloat16)
    d_gate = (d_act * up_pre * sigmoid_g * (1.0 + gate_pre * (1.0 - sigmoid_g))).astype(
        jnp.bfloat16
    )
    grad_gate = contract_rows(rows_x, d_gate).astype(jnp.bfloat16)
    grad_up = contract_rows(rows_x, d_up).astype(jnp.bfloat16)
    partial_value = (contract_cols(d_gate, gate_cols) + contract_cols(d_up, up_cols)).astype(
        jnp.bfloat16
    )
    returned = give_back(
        partial_value.reshape(2, experts, capacity, model_width), seq_devices, n_tp
    ).reshape(slot_count, quarter)
    stream_part = (source_g.astype(jnp.float32) + contract_rows(chosen, returned)).astype(
        jnp.bfloat16
    )
    aligned = model_width % (seq_devices * 128) == 0
    if aligned:
        stream, stream_block = share_stream(stream_part, halo, seq_devices, n_tp)
        grad_proj = contract_rows(
            stream_block.reshape(-1, stream_block.shape[2]),
            all_branch.reshape(-1, all_branch.shape[2]),
        )
    else:
        stream = lax.all_gather(stream_part, "tp", axis=1, tiled=True)
        grad_proj = lax.psum_scatter(
            contract_rows(stream, branch), "sp", scatter_dimension=0, tiled=True
        )
    d_branch = jnp.dot(stream, out_proj, preferred_element_type=jnp.float32)
    d_after = d_branch[tokens_here:]
    d_branch = d_branch[:tokens_here]
    grad_gate_b = (d_branch * conv_out.astype(jnp.float32)).astype(jnp.bfloat16)
    d_conv = d_branch * gate_b.astype(jnp.float32)
    kernel_taps = conv_taps.shape[0]
    kernel_reach = kernel_taps - 1
    if aligned:
        last = lax.axis_index("sp") == seq_devices - 1
        next_rows_in = jnp.where(last, 0.0, d_after * next_gate_b.astype(jnp.float32))[:kernel_reach]
    else:
        next_rows_in = from_behind(d_conv[:kernel_reach], "sp", -1)
    extended = jnp.concatenate([d_conv, next_rows_in], axis=0)
    d_input = jnp.zeros_like(d_conv)
    for tap_index in range(kernel_taps):
        offset = kernel_reach - tap_index
        d_input = d_input + conv_taps[tap_index][None, :] * extended[offset : offset + tokens_here]
    grad_hidden = (d_input * gate_c.astype(jnp.float32)).astype(jnp.bfloat16)
    grad_gate_c = (d_input * hidden_h.astype(jnp.float32)).astype(jnp.bfloat16)
    return (grad_gate, grad_up, grad_down, grad_proj, grad_hidden, grad_gate_b, grad_gate_c)


def solution(mesh):
    placed = (
        P("sp", None),
        P("sp", None),
        P("sp", None),
        P("sp", None),
        P(None, ("sp", "tp")),
        P(None, ("sp", "tp")),
        P(("sp", "tp"), None),
        P(None, "tp"),
        P("sp", "tp"),
        P("sp", "tp"),
        P("sp", "tp"),
        P("sp", "tp"),
        P(None, "tp"),
    )
    return jax.shard_map(
        per_device,
        mesh=mesh,
        in_specs=placed,
        out_specs=(
            P(None, ("sp", "tp")),
            P(None, ("sp", "tp")),
            P(("sp", "tp"), None),
            P("sp", "tp"),
            P("sp", "tp"),
            P("sp", "tp"),
            P("sp", "tp"),
        ),
        check_vma=False,
    )
```

profile of v0, /device:TPU:0, one launch (start us, length us, event | category | flops | bytes accessed | tf_op | source)
XLA Modules:
  0.0 125.5 jit_solution(4105687804492619689)
XLA Ops:
  0.6 0.0 copy-start
  0.6 0.9 copy.33
  1.6 0.1 eq.32
  1.7 0.2 fusion.3
  1.9 0.1 convert_element_type.74
  2.1 0.1 copy.34
  2.1 0.7 multiply_add_fusion
  2.9 1.2 convolution_convert_fusion.3
  4.1 0.8 select_reduce_fusion
  4.9 1.2 fusion.1
  6.1 0.8 fusion.12.branch_ref
  6.8 0.7 slice.27.head_ref
  7.5 41.3 %shard_map.180 = (bf16[2,4,96,2048]{3,2,1,0:T(8,128)(2,1)S(1)}, bf16[2,4,96,2048]{3,2,1,0:T(8,128)(2,1)}, bf16[8,128,128]{2,1,0:T(8,128)(2,1)S(1)}, bf16[16,128]{1,0:T(8,128)(2,1)S(1)}) custom-call(bf16[4,96,512]{2,1,0:T(8,128)(2,1)S(1)} %bitcast.39, bf16[4,96,512]{2,1,0:T(8,128)(2,1)S(1)} %bitcast.40, bf16[128,128]{1,0:T(8,128)(2,1)S(1)} %fusion.12.branch_ref, ...), custom_call_target="tpu_custom_call" | custom-call | tf_op jit(solution)/shard_map/pallas_call | solution.py:167
  48.9 1.6 %fusion.22 = f32[768,448]{0,1:T(8,128)S(1)} fusion(bf16[768,2048]{1,0:T(8,128)(2,1)S(1)} %bitcast.41, bf16[2048,448]{0,1:T(8,128)(2,1)S(1)} %copy-done), kind=kOutput, calls=%fused_computation.50 | convolution fusion | flops 1409286144 | bytes 6356992 | tf_op jit(solution)/shard_map/dot_general | solution.py:470
  50.5 0.0 copy-start.8
  50.5 1.6 %fusion.21 = f32[768,448]{0,1:T(8,128)S(1)} fusion(bf16[768,2048]{1,0:T(8,128)(2,1)S(1)} %bitcast.42, bf16[2048,448]{0,1:T(8,128)(2,1)S(1)} %copy-done.9), kind=kOutput, calls=%fused_computation.49 | convolution fusion | flops 1409286144 | bytes 6356992 | tf_op jit(solution)/shard_map/dot_general | solution.py:471
  52.2 0.2 copy-done.7
  52.4 0.6 copy-done.8
  53.0 2.0 %multiply_convert_fusion.1 = (bf16[768,448]{0,1:T(8,128)(2,1)S(1)}, bf16[768,448]{0,1:T(8,128)(2,1)S(1)}) fusion(f32[768,448]{0,1:T(8,128)S(1)} %fusion.22, f32[768,448]{0,1:T(8,128)S(1)} %fusion.21, bf16[768,2048]{1,0:T(8,128)(2,1)S(1)} %bitcast.45, bf16[448,2048]{1,0:T(8,128)(2,1)S(1)} %copy-done.8), kind=kOutput, calls=%fused_computation.5 | convolution fusion | flops 1413758976 | bytes 9109504 | tf_op jit(solution)/shard_map/dot_general | solution.py:418
  55.0 2.8 %convolution_convert_fusion.1 = bf16[2048,448]{0,1:T(8,128)(2,1)} fusion(bf16[768,448]{0,1:T(8,128)(2,1)S(1)} %get-tuple-element.22, bf16[768,2048]{1,0:T(8,128)(2,1)S(1)} %bitcast.43), kind=kOutput, calls=%fused_computation.2 | convolution fusion | flops 1410203648 | bytes 5668864 | tf_op jit(solution)/shard_map/dot_general | solution.py:412
  57.8 2.8 %convolution_convert_fusion = bf16[2048,448]{0,1:T(8,128)(2,1)} fusion(bf16[768,448]{0,1:T(8,128)(2,1)S(1)} %get-tuple-element.21, bf16[768,2048]{1,0:T(8,128)(2,1)S(1)} %bitcast.44), kind=kOutput, calls=%fused_computation.1 | convolution fusion | flops 1410203648 | bytes 5668864 | tf_op jit(solution)/shard_map/dot_general | solution.py:412
  60.7 2.9 %convolution_convert_fusion.2 = bf16[448,2048]{1,0:T(8,128)(2,1)} fusion(bf16[768,2048]{1,0:T(8,128)(2,1)S(1)} %bitcast.46, f32[768,448]{0,1:T(8,128)S(1)} %fusion.21, f32[768,448]{0,1:T(8,128)S(1)} %fusion.22), kind=kOutput, calls=%fused_computation.3 | convolution fusion | flops 1412268032 | bytes 7733248 | tf_op jit(solution)/shard_map/dot_general | solution.py:412
  63.5 1.8 %fusion.23 = f32[768,2048]{1,0:T(8,128)S(1)} fusion(bf16[768,448]{0,1:T(8,128)(2,1)S(1)} %get-tuple-element.22, bf16[2048,448]{0,1:T(8,128)(2,1)S(1)} %copy-done), kind=kOutput, calls=%fused_computation.51 | convolution fusion | flops 1409286144 | bytes 8814592 | tf_op jit(solution)/shard_map/dot_general | solution.py:418
  65.4 2.0 %add_convert_fusion = bf16[768,2048]{1,0:T(8,128)(2,1)S(1)} fusion(f32[768,2048]{1,0:T(8,128)S(1)} %fusion.23, bf16[768,448]{0,1:T(8,128)(2,1)S(1)} %get-tuple-element.21, bf16[2048,448]{0,1:T(8,128)(2,1)S(1)} %copy-done.9), kind=kOutput, calls=%fused_computation | convolution fusion | flops 1412431872 | bytes 11960320 | tf_op jit(solution)/shard_map/dot_general | solution.py:418
  67.4 29.4 %shard_map.181 = bf16[4,96,512]{2,1,0:T(8,128)(2,1)S(1)} custom-call(bf16[2,4,96,2048]{3,2,1,0:T(8,128)(2,1)S(1)} %bitcast.37), custom_call_target="tpu_custom_call" | custom-call | tf_op jit(solution)/shard_map/pallas_call | solution.py:290
  96.9 1.9 %fusion.2.part_ref = bf16[128,512]{1,0:T(8,128)(2,1)} fusion(pred[384,128]{1,0:T(8,128)(4,1)S(1)} %fusion.4, bf16[384,512]{1,0:T(8,128)(2,1)S(1)} %bitcast.38, bf16[128,2048]{1,0:T(8,128)(2,1)} %param.14, s32[]{:T(128)S(6)} %select_n.21), kind=kOutput, calls=%fused_computation.13 | convolution fusion | flops 50528256 | bytes 704516 | tf_op jit(solution)/shard_map/dot_general | solution.py:412
  98.8 21.3 %shard_map.182 = (bf16[144,2048]{1,0:T(8,128)(2,1)}, bf16[8,128,256]{2,1,0:T(8,128)(2,1)}) custom-call(bf16[128,512]{1,0:T(8,128)(2,1)} %fusion.2.part_ref), custom_call_target="tpu_custom_call" | custom-call | tf_op jit(solution)/shard_map/pallas_call | solution.py:383
  120.1 2.0 %convolution_bitcast_fusion = f32[256,128]{1,0:T(8,128)} fusion(bf16[8,128,256]{2,1,0:T(8,128)(2,1)} %get-tuple-element.15, bf16[8,128,128]{2,1,0:T(8,128)(2,1)S(1)} %get-tuple-element.16), kind=kOutput, calls=%fused_computation.14 | convolution fusion | flops 67108864 | bytes 917504 | tf_op jit(solution)/shard_map/dot_general | solution.py:412
  122.2 1.4 %fusion.24 = f32[144,128]{1,0:T(8,128)S(1)} fusion(bf16[144,2048]{1,0:T(8,128)(2,1)} %get-tuple-element.17, bf16[2048,128]{1,0:T(8,128)(2,1)S(1)} %copy-done.1), kind=kOutput, calls=%fused_computation.52 | convolution fusion | flops 75497472 | bytes 1187840 | tf_op jit(solution)/shard_map/dot_general | solution.py:504
  123.6 0.6 fusion.13
  124.2 0.7 multiply_convert_fusion.4
  124.9 0.6 multiply_convert_fusion.5
  (21 shorter events, 0.1 us)
Async XLA Ops:
  0.6 48.2 %copy-start = (bf16[2048,448]{0,1:T(8,128)(2,1)S(1)}, bf16[2048,448]{0,1:T(8,128)(2,1)}, u32[]{:S(2)}) copy-start(bf16[2048,448]{0,1:T(8,128)(2,1)} %param.17) | copy-start | bytes 5505028
  48.9 1.7 %copy-start.9 = (bf16[2048,448]{0,1:T(8,128)(2,1)S(1)}, bf16[2048,448]{0,1:T(8,128)(2,1)}, u32[]{:S(2)}) copy-start(bf16[2048,448]{0,1:T(8,128)(2,1)} %param.18) | copy-start | bytes 5505028
  50.5 1.9 %copy-start.7 = (bf16[2,4,96,2048]{3,2,1,0:T(8,128)(2,1)S(1)}, bf16[2,4,96,2048]{3,2,1,0:T(8,128)(2,1)}, u32[]{:S(2)}) copy-start(bf16[2,4,96,2048]{3,2,1,0:T(8,128)(2,1)} %get-tuple-element.14) | copy-start | bytes 9437188
  50.5 2.4 %copy-start.8 = (bf16[448,2048]{1,0:T(8,128)(2,1)S(1)}, bf16[448,2048]{1,0:T(8,128)(2,1)}, u32[]{:S(2)}) copy-start(bf16[448,2048]{1,0:T(8,128)(2,1)} %param.19) | copy-start | bytes 5505028
  67.4 54.7 %copy-start.1 = (bf16[2048,128]{1,0:T(8,128)(2,1)S(1)}, bf16[2048,128]{1,0:T(8,128)(2,1)}, u32[]{:S(2)}) copy-start(bf16[2048,128]{1,0:T(8,128)(2,1)} %param.20) | copy-start | bytes 1572868
  96.8 26.7 %copy-start.2 = (bf16[128,128]{1,0:T(8,128)(2,1)S(1)}, bf16[128,128]{1,0:T(8,128)(2,1)}, u32[]{:S(2)}) copy-start(bf16[128,128]{1,0:T(8,128)(2,1)} %param.22) | copy-start | bytes 98308
  96.9 26.7 %copy-start.3 = (bf16[128,128]{1,0:T(8,128)(2,1)S(1)}, bf16[128,128]{1,0:T(8,128)(2,1)}, u32[]{:S(2)}) copy-start(bf16[128,128]{1,0:T(8,128)(2,1)} %param.21) | copy-start | bytes 98308
  96.9 27.3 %copy-start.6 = (f32[3,128]{1,0:T(4,128)S(1)}, f32[3,128]{1,0:T(4,128)}, u32[]{:S(2)}) copy-start(f32[3,128]{1,0:T(4,128)} %param.25) | copy-start | bytes 4612
  96.9 27.3 %copy-start.4 = (bf16[128,128]{1,0:T(8,128)(2,1)S(1)}, bf16[128,128]{1,0:T(8,128)(2,1)}, u32[]{:S(2)}) copy-start(bf16[128,128]{1,0:T(8,128)(2,1)} %param.24) | copy-start | bytes 98308
  96.9 28.0 %copy-start.5 = (bf16[128,128]{1,0:T(8,128)(2,1)S(1)}, bf16[128,128]{1,0:T(8,128)(2,1)}, u32[]{:S(2)}) copy-start(bf16[128,128]{1,0:T(8,128)(2,1)} %param.23) | copy-start | bytes 98308
where the time goes:
time: 126 us
  Pallas kernels  92 us (73%)
  matrix products  25.5 us (20%)
  other arithmetic  4.29 us (3%)
  local copies, waits for them, and re-layouts  2.79 us (2%)
    pallas_call x1, Pallas kernels, dispatch(): pl.pallas_call(functools.partial(dispatch_kernel, n_sp, n_tp, chunks), ou...  41.3 us
    pallas_call x1, Pallas kernels, give_back(): pl.pallas_call(functools.partial(return_kernel, n_sp, n_tp, chunks), out_...  29.4 us
    pallas_call x1, Pallas kernels, share_stream(): pl.pallas_call(functools.partial(stream_kernel, n_sp, n_tp), out_shape=(j...  21.3 us
    dot_general x5, matrix products, contract_rows(): lax.dot_general(left_side, right_side, (((0,), (0,)), ((), ())), preferre...  12.4 us
    dot_general x3, matrix products, contract_cols(): lax.dot_general(left_side, right_side, (((1,), (1,)), ((), ())), preferre...  5.91 us

commit v1 on v0

--- a/solution.py
+++ b/solution.py
@@ -304,6 +304,278 @@
     )(part)
 
 
+def dot(left, right, left_dim, right_dim):
+    return lax.dot_general(
+        left, right, (((left_dim,), (right_dim,)), ((), ())), preferred_element_type=jnp.float32
+    )
+
+
+def flipped(index, bits):
+    bit = 1
+    while bit <= bits:
+        if bits & bit:
+            index = index + bit - 2 * bit * lax.rem(index // bit, 2)
+        bit *= 2
+    return index
+
+
+def expert_kernel(
+    n_sp, n_tp,
+    sent_x, sent_g, own_x, own_g, branch_ref, head_ref, wg, wu, wd,
+    out_back, out_b, out_head, out_gate, out_up, out_down,
+    rows_x, rows_g, act, dup, dgt, part_out, part_mine, from_pair, summed,
+    near_x, near_y, passed, far_x, far_y, final,
+    z_send, z_recv, own_send, own_recv, line_send, line_recv, relay_send, relay_recv,
+    pair_send, pair_recv, own_pair_send, own_pair_recv, b_send, b_recv, h_send, h_recv,
+    rp_send, rp_recv, near_send, near_recv, far_send, far_recv, back_send, back_recv,
+):
+    experts = n_sp // 2
+    sp, tp, expert, parity, row, core = place(n_tp)
+    capacity, width = sent_x.shape[1:]
+    model_width = own_x.shape[1]
+    wide = model_width // 2
+    half = width // 2
+    x_side = (2 * expert + 1 - parity, tp)
+    y_side = (sp, 2 * (1 - row) + core)
+    pair = (sp, 2 * row + 1 - core)
+    other_quarter = 2 * (1 - row) + core
+    sources, owned, rows = (sent_x, sent_g), (own_x, own_g), (rows_x, rows_g)
+    started = []
+
+    def send(src, dst, send_sem, recv_sem, device):
+        copy = pltpu.make_async_remote_copy(
+            src_ref=src, dst_ref=dst, send_sem=send_sem, recv_sem=recv_sem,
+            device_id=device, device_id_type=MESH,
+        )
+        copy.start()
+        started.append(copy)
+
+    def spot(t, j, par, quarter):
+        return rows[t].at[flipped(expert, j), par, :, columns(quarter, width)]
+
+    def side(t, par, which):
+        return rows[t].at[expert, par, :, columns(which, wide)]
+
+    greet([(lax.rem(sp + d, n_sp), tp) for d in range(1, n_sp)] + [y_side, pair])
+    order = [1] + list(range(experts - 1, 1, -1))
+    steps = [(j, t) for j in order for t in range(2)]
+    for j, t in steps:
+        target = flipped(expert, j)
+        send(sources[t].at[target], rows[t].at[expert, parity, :, columns(tp, width)],
+             z_send.at[t, j], z_recv.at[t, j], (2 * target + parity, tp))
+    for t in range(2):
+        send(owned[t].at[:, columns(core, wide)], side(t, parity, core), own_send.at[t], own_recv.at[t], x_side)
+    for t in range(2):
+        rows[t][expert, parity] = owned[t][...]
+
+    def own_stage(n):
+        j, t = steps[n]
+        block = spot(t, j, parity, tp)
+        wait_arrival(block, z_recv.at[t, j])
+        send(block, block, line_send.at[t, j, 0], line_recv.at[t, j, 0], x_side)
+        send(block, block, line_send.at[t, j, 1], line_recv.at[t, j, 1], y_side)
+        send(block, block, pair_send.at[t, j, 0], pair_recv.at[t, j, 0], pair)
+
+    def across_stage(t):
+        block = side(t, 1 - parity, core)
+        wait_arrival(block, own_recv.at[t])
+        send(block, block, own_pair_send.at[t], own_pair_recv.at[t], pair)
+
+    def near_x_stage(n):
+        j, t = steps[n]
+        block = spot(t, j, 1 - parity, tp)
+        wait_arrival(block, line_recv.at[t, j, 0])
+        if n % 3:
+            send(block, block, relay_send.at[t, j], relay_recv.at[t, j], y_side)
+        send(block, block, pair_send.at[t, j, 1], pair_recv.at[t, j, 1], pair)
+
+    def near_y_stage(n):
+        j, t = steps[n]
+        block = spot(t, j, parity, other_quarter)
+        wait_arrival(block, line_recv.at[t, j, 1])
+        if n % 3 == 0:
+            send(block, block, relay_send.at[t, j], relay_recv.at[t, j], x_side)
+        send(block, block, pair_send.at[t, j, 2], pair_recv.at[t, j, 2], pair)
+
+    def far_stage(n):
+        j, t = steps[n]
+        block = spot(t, j, 1 - parity, other_quarter)
+        wait_arrival(block, relay_recv.at[t, j])
+        send(block, block, pair_send.at[t, j, 3], pair_recv.at[t, j, 3], pair)
+
+    def forward(j):
+        source = flipped(expert, j)
+        for t in range(2):
+            if j == 0:
+                wait_arrival(side(t, 1 - parity, 1 - core), own_pair_recv.at[t])
+                continue
+            quarters = (2 * row + 1 - core, 2 * (1 - row) + 1 - core)
+            spots = ((parity, quarters[0]), (1 - parity, quarters[0]),
+                     (parity, quarters[1]), (1 - parity, quarters[1]))
+            for n, (par, quarter) in enumerate(spots):
+                wait_arrival(spot(t, j, par, quarter), pair_recv.at[t, j, n])
+        x = rows_x[source].reshape(2 * capacity, model_width)
+        g = rows_g[source].reshape(2 * capacity, model_width)
+        gate = dot(x, wg[...], 1, 1)
+        up = dot(x, wu[...], 1, 1)
+        d_act = dot(g, wd[...], 1, 1)
+        s = jax.nn.sigmoid(gate)
+        silu = gate * s
+        act[source] = (silu * up).astype(jnp.bfloat16)
+        dup[source] = (d_act * silu).astype(jnp.bfloat16)
+        dgt[source] = (d_act * up * s * (1.0 + gate * (1.0 - s))).astype(jnp.bfloat16)
+
+    def backward(j):
+        source = flipped(expert, j)
+        for kept in range(2):
+            side_core = core if kept else 1 - core
+            store = part_mine if kept else part_out
+            for line in range(2):
+                cols = columns(2 * line + side_core, width)
+                value = (
+                    dot(dgt[source], wg[:, cols], 1, 0) + dot(dup[source], wu[:, cols], 1, 0)
+                ).astype(jnp.bfloat16)
+                for par in range(2):
+                    piece = value[par * capacity : (par + 1) * capacity]
+                    store[j, 0, par, line] = piece[:, :half]
+                    store[j, 1, par, line] = piece[:, half:]
+            if not kept:
+                send(part_out.at[j], from_pair.at[j], rp_send.at[j], rp_recv.at[j], pair)
+
+    def reduce_pair(j):
+        wait_arrival(from_pair.at[j], rp_recv.at[j])
+        total = part_mine[j].astype(jnp.float32) + from_pair[j].astype(jnp.float32)
+        summed[j] = total.astype(jnp.bfloat16)
+        send(summed.at[j, 0, 1 - parity], near_x.at[j], near_send.at[j, 0], near_recv.at[j, 0], x_side)
+        send(summed.at[j, 1, :, 1 - row], near_y.at[j], near_send.at[j, 1], near_recv.at[j, 1], y_side)
+
+    def reduce_near(j):
+        wait_arrival(near_x.at[j], near_recv.at[j, 0])
+        total = summed[j, 0, parity, 1 - row].astype(jnp.float32) + near_x[j, 1 - row].astype(jnp.float32)
+        passed[j, 0] = total.astype(jnp.bfloat16)
+        send(passed.at[j, 0], far_y.at[j], far_send.at[j, 0], far_recv.at[j, 0], y_side)
+        wait_arrival(near_y.at[j], near_recv.at[j, 1])
+        total = summed[j, 1, 1 - parity, row].astype(jnp.float32) + near_y[j, 1 - parity].astype(jnp.float32)
+        passed[j, 1] = total.astype(jnp.bfloat16)
+        send(passed.at[j, 1], far_x.at[j], far_send.at[j, 1], far_recv.at[j, 1], x_side)
+
+    def reduce_far(j):
+        wait_arrival(far_y.at[j], far_recv.at[j, 0])
+        wait_arrival(far_x.at[j], far_recv.at[j, 1])
+        left = summed[j, 0, parity, row].astype(jnp.float32) + near_x[j, row].astype(jnp.float32)
+        left = (left + far_y[j].astype(jnp.float32)).astype(jnp.bfloat16)
+        right = summed[j, 1, parity, row].astype(jnp.float32) + near_y[j, parity].astype(jnp.float32)
+        right = (right + far_x[j].astype(jnp.float32)).astype(jnp.bfloat16)
+        if j == 0:
+            out_back[expert, :, :half] = left
+            out_back[expert, :, half:] = right
+            return
+        final[j, :, :half] = left
+        final[j, :, half:] = right
+        target = flipped(expert, j)
+        send(final.at[j], out_back.at[expert], back_send.at[j], back_recv.at[j], (2 * target + parity, tp))
+
+    def weight_grad(out, left, right, pieces):
+        tile = model_width // pieces
+        lhs = left[...].reshape(-1, left.shape[-1])
+        for n in range(pieces):
+            rhs = right[..., n * tile : (n + 1) * tile].reshape(-1, tile)
+            out[:, n * tile : (n + 1) * tile] = dot(lhs, rhs, 0, 0).astype(jnp.bfloat16)
+
+    def share_branch():
+        out_b[sp] = branch_ref[...]
+        for d in range(1, n_sp):
+            send(branch_ref, out_b.at[sp], b_send.at[d], b_recv.at[d], (lax.rem(sp + d, n_sp), tp))
+        send(head_ref, out_head, h_send.at[0], h_recv.at[0], (lax.rem(sp + n_sp - 1, n_sp), tp))
+
+    def some(stage, *numbers):
+        for n in numbers:
+            if n < len(steps):
+                stage(n)
+
+    chunk = [0] + order
+    some(own_stage, 0, 1)
+    across_stage(0)
+    some(near_y_stage, 0, 1)
+    across_stage(1)
+    some(own_stage, 2, 3)
+    forward(0)
+    some(near_x_stage, 0, 1)
+    backward(0)
+    for i in range(1, experts):
+        n = 2 * i
+        some(near_y_stage, n, n + 1)
+        some(far_stage, n - 2, n - 1)
+        some(own_stage, n + 2, n + 3)
+        reduce_pair(chunk[i - 1])
+        if i == 2:
+            share_branch()
+        forward(chunk[i])
+        some(near_x_stage, n, n + 1)
+        reduce_near(chunk[i - 1])
+        backward(chunk[i])
+        reduce_far(chunk[i - 1])
+    if experts == 2:
+        share_branch()
+    last = chunk[-1]
+    reduce_pair(last)
+    weight_grad(out_down, act, rows_g, 4)
+    reduce_near(last)
+    weight_grad(out_gate, dgt, rows_x, 4)
+    reduce_far(last)
+    weight_grad(out_up, dup, rows_x, 4)
+    for j in order:
+        wait_arrival(out_back.at[flipped(expert, j)], back_recv.at[j])
+    for d in range(1, n_sp):
+        wait_arrival(out_b.at[lax.rem(sp + n_sp - d, n_sp)], b_recv.at[d])
+    wait_arrival(out_head, h_recv.at[0])
+    for copy in started:
+        copy.wait_send()
+
+
+def run_experts(sent_x, sent_g, own_x, own_g, branch, head, wg, wu, wd, n_sp, n_tp):
+    experts, capacity, width = sent_x.shape
+    model_width = own_x.shape[1]
+    units = wg.shape[0]
+    half = width // 2
+    dma = pltpu.SemaphoreType.DMA
+    bf16 = jnp.bfloat16
+
+    def out(*shape):
+        return jax.ShapeDtypeStruct(shape, bf16)
+
+    def vmem(*shape):
+        return pltpu.VMEM(shape, bf16)
+
+    rows = vmem(experts, 2, capacity, model_width)
+    hidden = vmem(experts, 2 * capacity, units)
+    blocks = vmem(experts, 2, 2, 2, capacity, half)
+    near = vmem(experts, 2, capacity, half)
+    far = vmem(experts, capacity, half)
+    return pl.pallas_call(
+        functools.partial(expert_kernel, n_sp, n_tp),
+        out_shape=(
+            out(experts, capacity, width), out(n_sp, *branch.shape), out(*head.shape),
+            out(units, model_width), out(units, model_width), out(units, model_width),
+        ),
+        in_specs=[VMEM] * 9,
+        out_specs=(VMEM,) * 6,
+        scratch_shapes=[
+            rows, rows, hidden, hidden, hidden, blocks, blocks, blocks, blocks,
+            near, near, near, far, far, vmem(experts, capacity, width),
+            dma((2, experts)), dma((2, experts)), dma((2,)), dma((2,)),
+            dma((2, experts, 2)), dma((2, experts, 2)), dma((2, experts)), dma((2, experts)),
+            dma((2, experts, 4)), dma((2, experts, 4)), dma((2,)), dma((2,)),
+            dma((n_sp,)), dma((n_sp,)), dma((1,)), dma((1,)),
+            dma((experts,)), dma((experts,)), dma((experts, 2)), dma((experts, 2)),
+            dma((experts, 2)), dma((experts, 2)), dma((experts,)), dma((experts,)),
+        ],
+        compiler_params=pltpu.CompilerParams(
+            collective_id=3, has_side_effects=True, vmem_limit_bytes=56 * 1024 * 1024
+        ),
+    )(sent_x, sent_g, own_x, own_g, branch, head, wg, wu, wd)
+
+
 def stream_kernel(
     n_sp, n_tp, part_ref, stream_ref, block_ref,
     tp_send, tp_recv, h_send, h_recv, b_send, b_recv, s_send, s_recv,
@@ -457,39 +729,65 @@
     sent_g = (slot_weight[:, None] * sent_g).astype(jnp.bfloat16)
     branch = (gate_b.astype(jnp.float32) * conv_out.astype(jnp.float32)).astype(jnp.bfloat16)
     halo = 16
-    rows_x, rows_g, all_branch, next_gate_b = dispatch(
-        sent_x.reshape(experts, capacity, quarter),
-        sent_g.reshape(experts, capacity, quarter),
-        branch,
-        gate_b[:halo],
-        seq_devices,
-        n_tp,
-    )
-    rows_x = rows_x.reshape(-1, model_width)
-    rows_g = rows_g.reshape(-1, model_width)
-    gate_pre = jnp.dot(rows_x, gate_cols, preferred_element_type=jnp.float32)
-    up_pre = jnp.dot(rows_x, up_cols, preferred_element_type=jnp.float32)
-    sigmoid_g = jax.nn.sigmoid(gate_pre)
-    silu_g = gate_pre * sigmoid_g
-    activation = (silu_g * up_pre).astype(jnp.bfloat16)
-    grad_down = contract_rows(activation, rows_g).astype(jnp.bfloat16)
-    d_act = contract_cols(rows_g, down_rows)
-    d_up = (d_act * silu_g).astype(jnp.bfloat16)
-    d_gate = (d_act * up_pre * sigmoid_g * (1.0 + gate_pre * (1.0 - sigmoid_g))).astype(
-        jnp.bfloat16
-    )
-    grad_gate = contract_rows(rows_x, d_gate).astype(jnp.bfloat16)
-    grad_up = contract_rows(rows_x, d_up).astype(jnp.bfloat16)
-    partial_value = (contract_cols(d_gate, gate_cols) + contract_cols(d_up, up_cols)).astype(
-        jnp.bfloat16
-    )
-    returned = give_back(
-        partial_value.reshape(2, experts, capacity, model_width), seq_devices, n_tp
-    ).reshape(slot_count, quarter)
+    aligned = model_width % (seq_devices * 128) == 0
+    if aligned:
+        own = lax.dynamic_slice_in_dim(
+            chosen, (lax.axis_index("sp") // 2) * capacity, capacity, 0
+        )
+        own_weight = lax.dynamic_slice_in_dim(
+            slot_weight, (lax.axis_index("sp") // 2) * capacity, capacity, 0
+        )
+        own_x = jnp.dot(own, moe_input, preferred_element_type=jnp.float32).astype(jnp.bfloat16)
+        own_g = jnp.dot(own, out_grad, preferred_element_type=jnp.float32)
+        own_g = (own_weight[:, None] * own_g).astype(jnp.bfloat16)
+        returned, all_branch, next_gate_b, grad_gate, grad_up, grad_down = run_experts(
+            sent_x.reshape(experts, capacity, quarter),
+            sent_g.reshape(experts, capacity, quarter),
+            own_x,
+            own_g,
+            branch,
+            gate_b[:halo],
+            gate_cols.T,
+            up_cols.T,
+            down_rows,
+            seq_devices,
+            n_tp,
+        )
+        returned = returned.reshape(slot_count, quarter)
+        grad_gate, grad_up = grad_gate.T, grad_up.T
+    else:
+        rows_x, rows_g, all_branch, next_gate_b = dispatch(
+            sent_x.reshape(experts, capacity, quarter),
+            sent_g.reshape(experts, capacity, quarter),
+            branch,
+            gate_b[:halo],
+            seq_devices,
+            n_tp,
+        )
+        rows_x = rows_x.reshape(-1, model_width)
+        rows_g = rows_g.reshape(-1, model_width)
+        gate_pre = jnp.dot(rows_x, gate_cols, preferred_element_type=jnp.float32)
+        up_pre = jnp.dot(rows_x, up_cols, preferred_element_type=jnp.float32)
+        sigmoid_g = jax.nn.sigmoid(gate_pre)
+        silu_g = gate_pre * sigmoid_g
+        activation = (silu_g * up_pre).astype(jnp.bfloat16)
+        grad_down = contract_rows(activation, rows_g).astype(jnp.bfloat16)
+        d_act = contract_cols(rows_g, down_rows)
+        d_up = (d_act * silu_g).astype(jnp.bfloat16)
+        d_gate = (d_act * up_pre * sigmoid_g * (1.0 + gate_pre * (1.0 - sigmoid_g))).astype(
+            jnp.bfloat16
+        )
+        grad_gate = contract_rows(rows_x, d_gate).astype(jnp.bfloat16)
+        grad_up = contract_rows(rows_x, d_up).astype(jnp.bfloat16)
+        partial_value = (contract_cols(d_gate, gate_cols) + contract_cols(d_up, up_cols)).astype(
+            jnp.bfloat16
+        )
+        returned = give_back(
+            partial_value.reshape(2, experts, capacity, model_width), seq_devices, n_tp
+        ).reshape(slot_count, quarter)
     stream_part = (source_g.astype(jnp.float32) + contract_rows(chosen, returned)).astype(
         jnp.bfloat16
     )
-    aligned = model_width % (seq_devices * 128) == 0
     if aligned:
         stream, stream_block = share_stream(stream_part, halo, seq_devices, n_tp)
         grad_proj = contract_rows(

time: 126 us -> 122 us (0.968)
  matrix products: 25.5 us -> 10.7 us
  local copies, waits for them, and re-layouts: 2.79 us -> 7.47 us
  Pallas kernels: 92 us -> 95 us
  other arithmetic: 4.29 us -> 7.07 us
    dot_general x5 -> x2, matrix products: 12.4 us -> 4.02 us  [contract_rows(): lax.dot_general(left_side, right_side, (((0,), (0,)), ((), ())), preferre...]
    dot_general x5 -> x2, matrix products: 9.18 us -> 3.08 us  [the longest x1 2.08 us: per_device(): own_g = jnp.dot(own, out_grad, preferred_element_type=jnp.float32)]
    unnamed x21 -> x24, local copies, waits for them, and re-layouts: 1.76 us -> 6.46 us
    pallas_call x2 -> x1, Pallas kernels: 70.7 us -> 74.2 us  [run_experts(): pl.pallas_call(functools.partial(expert_kernel, n_sp, n_tp), out_shape=(o...]
where the time goes in v1:
time: 122 us; the launch traced here: 121 us
  Pallas kernels  95 us (78%)
  matrix products  10.7 us (9%)
  local copies, waits for them, and re-layouts  7.47 us (6%)
  other arithmetic  7.07 us (6%)
    pallas_call x1, Pallas kernels, run_experts(): pl.pallas_call(functools.partial(expert_kernel, n_sp, n_tp), out_shape=(o...  74.2 us
    pallas_call x1, Pallas kernels, share_stream(): pl.pallas_call(functools.partial(stream_kernel, n_sp, n_tp), out_shape=(j...  20.9 us
    unnamed x24, local copies, waits for them, and re-layouts  6.46 us
    dot_general x2, matrix products, contract_rows(): lax.dot_general(left_side, right_side, (((0,), (0,)), ((), ())), preferre...  4.02 us

profile of v1, /device:TPU:0, one launch (start us, length us, event | category | flops | bytes accessed | tf_op | source)
XLA Modules:
  0.0 121.1 jit_solution(13787943296961211659)
XLA Ops:
  0.6 0.0 copy-start
  0.6 0.0 copy-start.4
  0.7 0.0 copy-start.7
  0.7 0.9 copy.33
  1.6 0.1 eq.32
  1.7 0.2 fusion.3
  1.9 0.1 convert_element_type.59
  2.1 0.1 copy.34
  2.1 0.7 multiply_add_fusion
  2.8 0.8 select_reduce_fusion
  3.7 0.1 dynamic_slice.15
  3.8 2.1 %fusion.own_g = bf16[96,2048]{1,0:T(8,128)(2,1)} fusion(bf16[128,2048]{1,0:T(8,128)(2,1)} %param.14, f32[96]{0:T(128)S(1)} %dynamic_slice.15, pred[384,128]{1,0:T(8,128)(4,1)S(1)} %fusion.4, s32[]{:T(128)S(6)} %select_n.34), kind=kOutput, calls=%fused_computation.1 | convolution fusion | flops 50724864 | bytes 930308 | tf_op jit(solution)/shard_map/dot_general | solution.py:741
  5.9 1.0 convolution_convert_fusion.own_x
  6.9 1.0 fusion.1
  7.9 1.0 convolution_convert_fusion.1
  8.9 0.6 fusion.11.branch_ref
  9.5 0.6 slice.27.head_ref
  10.1 74.2 %shard_map.180 = (bf16[4,96,512]{2,1,0:T(8,128)(2,1)}, bf16[8,128,128]{2,1,0:T(8,128)(2,1)}, bf16[16,128]{1,0:T(8,128)(2,1)}, bf16[448,2048]{1,0:T(8,128)(2,1)},...) custom-call(bf16[4,96,512]{2,1,0:T(8,128)(2,1)} %bitcast.30, bf16[4,96,512]{2,1,0:T(8,128)(2,1)} %bitcast.29, ...), custom_call_target="tpu_custom_call" | custom-call | tf_op jit(solution)/shard_map/pallas_call | solution.py:555
  84.3 0.0 copy-start.9
  84.3 2.1 %fusion.2.part_ref = bf16[128,512]{1,0:T(8,128)(2,1)} fusion(pred[384,128]{1,0:T(8,128)(4,1)S(1)} %fusion.4, bf16[384,512]{1,0:T(8,128)(2,1)} %bitcast.31, bf16[128,2048]{1,0:T(8,128)(2,1)S(1)} %copy-done.4, s32[]{:T(128)S(6)} %select_n.31), kind=kOutput, calls=%fused_computation.7 | convolution fusion | flops 50528256 | bytes 704516 | tf_op jit(solution)/shard_map/dot_general | solution.py:684
  86.4 20.9 %shard_map.181 = (bf16[144,2048]{1,0:T(8,128)(2,1)}, bf16[8,128,256]{2,1,0:T(8,128)(2,1)}) custom-call(bf16[128,512]{1,0:T(8,128)(2,1)} %fusion.2.part_ref), custom_call_target="tpu_custom_call" | custom-call | tf_op jit(solution)/shard_map/pallas_call | solution.py:655
  107.3 1.4 %fusion.23 = f32[144,128]{1,0:T(8,128)S(1)} fusion(bf16[144,2048]{1,0:T(8,128)(2,1)} %get-tuple-element.21, bf16[2048,128]{1,0:T(8,128)(2,1)S(1)} %copy-done.5), kind=kOutput, calls=%fused_computation.46 | convolution fusion | flops 75497472 | bytes 1187840 | tf_op jit(solution)/shard_map/dot_general | solution.py:802
  108.7 0.7 fusion.17
  109.4 1.4 %fusion.12 = (bf16[128,128]{1,0:T(8,128)(2,1)}, f32[128,128]{1,0:T(8,128)S(1)}) fusion(bf16[128,128]{1,0:T(8,128)(2,1)} %param.21, f32[144,128]{1,0:T(8,128)S(1)} %fusion.23, bf16[128,128]{1,0:T(8,128)(2,1)} %param.22), kind=kLoop, calls=%fused_computation.27 | loop fusion | flops 81920 | bytes 229376 | tf_op jit(solution)/shard_map/convert_element_type | solution.py:805
  110.8 1.4 %multiply_convert_fusion = (bf16[128,128]{1,0:T(8,128)(2,1)}, f32[128,128]{1,0:T(8,128)S(1)}) fusion(bf16[128,128]{1,0:T(8,128)(2,1)} %param.24, f32[128,128]{1,0:T(8,128)S(1)} %get-tuple-element.26, f32[128]{0:T(128)S(1)} %get-tuple-element.28, f32[2,128]{1,0:T(2,128)S(1)} %fusion.17, f32[128]{0:T(128)S(1)} %get-tuple-element.29, f32[128]{0:T(128)S(1)} %get-tuple-element.27), kind=kLoop, calls=%fused_computation.30 | loop fusion | flops 163840 | bytes 199168 | tf_op jit(solution)/shard_map/convert_element_type | solution.py:820
  112.2 1.4 %multiply_convert_fusion.1 = bf16[128,128]{1,0:T(8,128)(2,1)} fusion(f32[128,128]{1,0:T(8,128)S(1)} %get-tuple-element.24, bf16[128,128]{1,0:T(8,128)(2,1)} %param.23), kind=kLoop, calls=%fused_computation.31 | loop fusion | flops 49152 | bytes 131072 | tf_op jit(solution)/shard_map/convert_element_type | solution.py:819
  113.6 1.9 %convolution_bitcast_fusion = f32[256,128]{1,0:T(8,128)} fusion(bf16[8,128,256]{2,1,0:T(8,128)(2,1)S(1)} %copy-done.6, bf16[8,128,128]{2,1,0:T(8,128)(2,1)} %get-tuple-element.20), kind=kOutput, calls=%fused_computation.8 | convolution fusion | flops 67108864 | bytes 917504 | tf_op jit(solution)/shard_map/dot_general | solution.py:684
  115.6 1.2 %copy.40 = bf16[2048,448]{0,1:T(8,128)(2,1)} copy(bf16[2048,448]{0,1:T(8,128)(2,1)S(1)} %bitcast.26) | data formatting | bytes 3670016
  116.8 0.9 copy-done.2
  117.7 1.2 %copy.41 = bf16[2048,448]{0,1:T(8,128)(2,1)} copy(bf16[2048,448]{0,1:T(8,128)(2,1)S(1)} %bitcast.25) | data formatting | bytes 3670016
  118.9 0.9 copy-done.1
  119.9 1.2 %copy.42 = bf16[448,2048]{1,0:T(8,128)(2,1)} copy(bf16[448,2048]{1,0:T(8,128)(2,1)S(1)} %copy-done.1) | data formatting | bytes 3670016
  (18 shorter events, 0.1 us)
Async XLA Ops:
  0.6 5.2 %copy-start = (bf16[128,2048]{1,0:T(8,128)(2,1)S(1)}, bf16[128,2048]{1,0:T(8,128)(2,1)}, u32[]{:S(2)}) copy-start(bf16[128,2048]{1,0:T(8,128)(2,1)} %param.13) | copy-start | bytes 1572868
  0.6 6.2 %copy-start.4 = (bf16[128,2048]{1,0:T(8,128)(2,1)S(1)}, bf16[128,2048]{1,0:T(8,128)(2,1)}, u32[]{:S(2)}) copy-start(bf16[128,2048]{1,0:T(8,128)(2,1)} %param.14) | copy-start | bytes 1572868
  0.7 8.2 %copy-start.8 = (bf16[128,128]{1,0:T(8,128)(2,1)S(1)}, bf16[128,128]{1,0:T(8,128)(2,1)}, u32[]{:S(2)}) copy-start(bf16[128,128]{1,0:T(8,128)(2,1)} %param.21) | copy-start | bytes 98308
  0.7 8.2 %copy-start.7 = (bf16[128,128]{1,0:T(8,128)(2,1)S(1)}, bf16[128,128]{1,0:T(8,128)(2,1)}, u32[]{:S(2)}) copy-start(bf16[128,128]{1,0:T(8,128)(2,1)} %param.22) | copy-start | bytes 98308
  10.1 97.2 %copy-start.5 = (bf16[2048,128]{1,0:T(8,128)(2,1)S(1)}, bf16[2048,128]{1,0:T(8,128)(2,1)}, u32[]{:S(2)}) copy-start(bf16[2048,128]{1,0:T(8,128)(2,1)} %param.20) | copy-start | bytes 1572868
  84.3 26.5 %copy-start.9 = (f32[3,128]{1,0:T(4,128)S(1)}, f32[3,128]{1,0:T(4,128)}, u32[]{:S(2)}) copy-start(f32[3,128]{1,0:T(4,128)} %param.25) | copy-start | bytes 4612
  84.3 31.3 %copy-start.3 = (bf16[448,2048]{1,0:T(8,128)(2,1)S(1)}, bf16[448,2048]{1,0:T(8,128)(2,1)}, u32[]{:S(2)}) copy-start(bf16[448,2048]{1,0:T(8,128)(2,1)} %get-tuple-element.15) | copy-start | bytes 5505028
  107.3 6.3 %copy-start.6 = (bf16[8,128,256]{2,1,0:T(8,128)(2,1)S(1)}, bf16[8,128,256]{2,1,0:T(8,128)(2,1)}, u32[]{:S(2)}) copy-start(bf16[8,128,256]{2,1,0:T(8,128)(2,1)} %get-tuple-element.19) | copy-start | bytes 1572868
  115.6 2.2 %copy-start.2 = (bf16[448,2048]{1,0:T(8,128)(2,1)S(1)}, bf16[448,2048]{1,0:T(8,128)(2,1)}, u32[]{:S(2)}) copy-start(bf16[448,2048]{1,0:T(8,128)(2,1)} %get-tuple-element.16) | copy-start | bytes 5505028
  117.7 2.2 %copy-start.1 = (bf16[448,2048]{1,0:T(8,128)(2,1)S(1)}, bf16[448,2048]{1,0:T(8,128)(2,1)}, u32[]{:S(2)}) copy-start(bf16[448,2048]{1,0:T(8,128)(2,1)} %get-tuple-element.39) | copy-start | bytes 5505028

commit v2 on v0

--- a/solution.py
+++ b/solution.py
@@ -16,6 +16,7 @@
 
 MESH = pl.DeviceIdType.MESH
 VMEM = pl.BlockSpec(memory_space=pltpu.VMEM)
+ANY = pl.BlockSpec(memory_space=pl.ANY)
 
 
 def columns(index, width):
@@ -304,6 +305,457 @@
     )(part)
 
 
+def dot(left, right, left_dim, right_dim):
+    return lax.dot_general(
+        left, right, (((left_dim,), (right_dim,)), ((), ())), preferred_element_type=jnp.float32
+    )
+
+
+def flipped(index, bits):
+    bit = 1
+    while bit <= bits:
+        if bits & bit:
+            index = index + bit - 2 * bit * lax.rem(index // bit, 2)
+        bit *= 2
+    return index
+
+
+PLAN_CHUNKS = (1, 3, 2)
+PLAN_OVER_X = (0, 4,)
+PLAN = (
+    ("depart", 1), ("cross", 0, 1), ("cross", 0, 0), ("depart", 2), ("own", 1), ("cross", 1, 1),
+    ("depart", 0), ("depart", 3), ("own", 0), ("across", 0, 0), ("depart", 4), ("own", 2), ("near_y", 0),
+    ("near_x", 1), ("near_x", 0), ("own", 3), ("across", 0, 1), ("depart", 5), ("near_y", 1),
+    ("across", 1, 1), ("far", 1), ("near_x", 2), ("far", 0), ("own", 4), ("pre", 1), ("near_y", 2),
+    ("near_x", 3), ("hidden", 1), ("far", 2), ("own", 5), ("pre", 0), ("near_x", 4), ("back", 1),
+    ("near_y", 4), ("pre", 3), ("near_y", 3), ("cross", 1, 0), ("far", 3), ("near_x", 5), ("pair", 1),
+    ("hidden", 3), ("far", 4), ("back", 3), ("pre", 2), ("near_y", 5), ("far", 5), ("pair", 3), ("hidden", 2),
+    ("fold_x", 1), ("across", 1, 0), ("fold_y", 1), ("back", 2), ("fold_x", 3), ("fold_y", 3), ("pair", 2),
+    ("home", 1), ("hidden", 0), ("back", 0), ("home", 3), ("fold_y", 2), ("fold_x", 2), ("grad", 6),
+    ("pair", 0), ("grad", 5), ("grad", 8), ("home", 2), ("grad", 2), ("grad", 3), ("grad", 0), ("grad", 9),
+    ("fold_x", 0), ("fold_y", 0), ("grad", 11), ("grad", 7), ("grad", 4), ("grad", 10), ("grad", 1),
+    ("home", 0),
+)
+
+
+def expert_kernel(
+    n_sp, n_tp,
+    chosen_ref, weight_ref, token_x, token_g, gate_b, conv_out, gate_ref, up_ref, down_ref,
+    stream_ref, block_ref, out_b, out_head, out_gate, out_up, out_down,
+    sent_x, sent_g, out_back, part_ref,
+    rows_x, rows_g, act, dup, dgt, part_out, part_mine, from_pair, summed,
+    near_x, near_y, passed, far_x, far_y, final, wg, wu, wd, gate_pre, up_pre,
+    w_sem, z_send, z_recv, own_send, own_recv, line_send, line_recv, relay_send, relay_recv,
+    pair_send, pair_recv, own_pair_send, own_pair_recv, b_send, b_recv, h_send, h_recv,
+    rp_send, rp_recv, near_send, near_recv, far_send, far_recv, back_send, back_recv,
+    gather_send, gather_recv, halo_send, halo_recv, place_send, place_recv, held_send, held_recv,
+):
+    experts = n_sp // 2
+    sp, tp, expert, parity, row, core = place(n_tp)
+    capacity, width = sent_x.shape[1:]
+    tokens, model_width = token_x.shape
+    half = width // 2
+    halo = out_head.shape[0]
+    x_side = (2 * expert + 1 - parity, tp)
+    y_side = (sp, 2 * (1 - row) + core)
+    pair = (sp, 2 * row + 1 - core)
+    other_quarter = 2 * (1 - row) + core
+    sources, rows = (sent_x, sent_g), (rows_x, rows_g)
+    started = []
+
+    def send(src, dst, send_sem, recv_sem, device):
+        copy = pltpu.make_async_remote_copy(
+            src_ref=src, dst_ref=dst, send_sem=send_sem, recv_sem=recv_sem,
+            device_id=device, device_id_type=MESH,
+        )
+        copy.start()
+        started.append(copy)
+
+    def spot(t, j, par, quarter):
+        return rows[t].at[flipped(expert, j), par, :, columns(quarter, width)]
+
+    loads = [
+        pltpu.make_async_copy(src, dst, w_sem.at[n])
+        for n, (src, dst) in enumerate(((gate_ref, wg), (up_ref, wu), (down_ref, wd)))
+    ]
+    for load in loads:
+        load.start()
+    before, after = lax.rem(sp + n_sp - 1, n_sp), lax.rem(sp + 1, n_sp)
+    fixed = [x_side, y_side, pair] + [(2 * flipped(expert, j) + parity, tp) for j in PLAN_CHUNKS]
+    fixed += [(near, (lax.rem(tp + n, n_tp))) for near in (before, after) for n in range(n_tp)]
+    targets = [(2 * (core + 2 * h) + row, expert) for h in range(2)]
+    origins = [(2 * tp + par, 2 * parity + lax.rem(expert, 2)) for par in range(2)]
+    barrier = pltpu.get_barrier_semaphore()
+    for peer in fixed:
+        pl.semaphore_signal(barrier, inc=1, device_id=peer, device_id_type=MESH)
+    expected = len(fixed)
+    for peer in targets + origins:
+        away = jnp.logical_or(peer[0] != sp, peer[1] != tp)
+
+        @pl.when(away)
+        def _(peer=peer):
+            pl.semaphore_signal(barrier, inc=1, device_id=peer, device_id_type=MESH)
+
+        expected = expected + away.astype(jnp.int32)
+    out_b[parity, expert] = (
+        gate_b[...].astype(jnp.float32) * conv_out[...].astype(jnp.float32)
+    ).astype(jnp.bfloat16)
+    slot_weight = jnp.sum(weight_ref[...], axis=2, keepdims=True)
+    mine = columns(tp, width)
+    one_hot = chosen_ref[...].reshape(experts * capacity, tokens)
+    sent_x[...] = dot(one_hot, token_x[:, mine], 1, 0).astype(jnp.bfloat16).reshape(sent_x.shape)
+    scaled = slot_weight * dot(one_hot, token_g[:, mine], 1, 0).reshape(sent_g.shape)
+    sent_g[...] = scaled.astype(jnp.bfloat16)
+    one_hot = chosen_ref[expert]
+    slot_weight = jnp.sum(weight_ref[expert], axis=1, keepdims=True)
+    rows_x[expert, parity] = dot(one_hot, token_x[...], 1, 0).astype(jnp.bfloat16)
+    rows_g[expert, parity] = (slot_weight * dot(one_hot, token_g[...], 1, 0)).astype(jnp.bfloat16)
+    pl.semaphore_wait(barrier, expected)
+    steps = [(j, t) for j in PLAN_CHUNKS for t in range(2)]
+
+    def depart(n):
+        j, t = steps[n]
+        target = flipped(expert, j)
+        send(sources[t].at[target], rows[t].at[expert, parity, :, columns(tp, width)],
+             z_send.at[t, j], z_recv.at[t, j], (2 * target + parity, tp))
+
+    def piece(t, par, which, part):
+        return rows[t].at[expert, par, :, columns(2 * which + part, width)]
+
+    def cross(t, part):
+        block = piece(t, parity, core, part)
+        send(block, block, own_send.at[t, part], own_recv.at[t, part], x_side)
+
+    def own_stage(n):
+        j, t = steps[n]
+        block = spot(t, j, parity, tp)
+        wait_arrival(block, z_recv.at[t, j])
+        send(block, block, line_send.at[t, j, 0], line_recv.at[t, j, 0], x_side)
+        send(block, block, line_send.at[t, j, 1], line_recv.at[t, j, 1], y_side)
+        send(block, block, pair_send.at[t, j, 0], pair_recv.at[t, j, 0], pair)
+
+    def across_stage(t, part):
+        block = piece(t, 1 - parity, core, part)
+        wait_arrival(block, own_recv.at[t, part])
+        send(block, block, own_pair_send.at[t, part], own_pair_recv.at[t, part], pair)
+
+    def near_x_stage(n):
+        j, t = steps[n]
+        block = spot(t, j, 1 - parity, tp)
+        wait_arrival(block, line_recv.at[t, j, 0])
+        if n not in PLAN_OVER_X:
+            send(block, block, relay_send.at[t, j], relay_recv.at[t, j], y_side)
+        send(block, block, pair_send.at[t, j, 1], pair_recv.at[t, j, 1], pair)
+
+    def near_y_stage(n):
+        j, t = steps[n]
+        block = spot(t, j, parity, other_quarter)
+        wait_arrival(block, line_recv.at[t, j, 1])
+        if n in PLAN_OVER_X:
+            send(block, block, relay_send.at[t, j], relay_recv.at[t, j], x_side)
+        send(block, block, pair_send.at[t, j, 2], pair_recv.at[t, j, 2], pair)
+
+    def far_stage(n):
+        j, t = steps[n]
+        block = spot(t, j, 1 - parity, other_quarter)
+        wait_arrival(block, relay_recv.at[t, j])
+        send(block, block, pair_send.at[t, j, 3], pair_recv.at[t, j, 3], pair)
+
+    def arrived(j, t):
+        if j == 0:
+            for part in range(2):
+                wait_arrival(piece(t, 1 - parity, 1 - core, part), own_pair_recv.at[t, part])
+            return
+        quarters = (2 * row + 1 - core, 2 * (1 - row) + 1 - core)
+        spots = ((parity, quarters[0]), (1 - parity, quarters[0]),
+                 (parity, quarters[1]), (1 - parity, quarters[1]))
+        for n, (par, quarter) in enumerate(spots):
+            wait_arrival(spot(t, j, par, quarter), pair_recv.at[t, j, n])
+
+    def pre_stage(j):
+        arrived(j, 0)
+        if waiting:
+            for load in waiting:
+                load.wait()
+            waiting.clear()
+        x = rows_x[flipped(expert, j)].reshape(2 * capacity, model_width)
+        gate_pre[j] = dot(x, wg[...], 1, 1)
+        up_pre[j] = dot(x, wu[...], 1, 1)
+
+    def hidden_stage(j):
+        arrived(j, 1)
+        source = flipped(expert, j)
+        g = rows_g[source].reshape(2 * capacity, model_width)
+        d_act = dot(g, wd[...], 1, 1)
+        gate, up = gate_pre[j], up_pre[j]
+        s = jax.nn.sigmoid(gate)
+        silu = gate * s
+        act[source] = (silu * up).astype(jnp.bfloat16)
+        dup[source] = (d_act * silu).astype(jnp.bfloat16)
+        dgt[source] = (d_act * up * s * (1.0 + gate * (1.0 - s))).astype(jnp.bfloat16)
+
+    def backward(j):
+        source = flipped(expert, j)
+        for kept in range(2):
+            side_core = core if kept else 1 - core
+            store = part_mine if kept else part_out
+            for h in range(2):
+                cols = columns(2 * h + side_core, width)
+                value = (
+                    dot(dgt[source], wg[:, cols], 1, 0) + dot(dup[source], wu[:, cols], 1, 0)
+                ).astype(jnp.bfloat16)
+                for par in range(2):
+                    piece = value[par * capacity : (par + 1) * capacity]
+                    store[j, h, par, 0] = piece[:, :half]
+                    store[j, h, par, 1] = piece[:, half:]
+            if not kept:
+                send(part_out.at[j], from_pair.at[j], rp_send.at[j], rp_recv.at[j], pair)
+
+    def reduce_pair(j):
+        wait_arrival(from_pair.at[j], rp_recv.at[j])
+        total = part_mine[j].astype(jnp.float32) + from_pair[j].astype(jnp.float32)
+        summed[j] = total.astype(jnp.bfloat16)
+        send(summed.at[j, 0, 1 - parity], near_x.at[j], near_send.at[j, 0], near_recv.at[j, 0], x_side)
+        send(summed.at[j, 1, :, 1 - row], near_y.at[j], near_send.at[j, 1], near_recv.at[j, 1], y_side)
+
+    def fold_x(j):
+        wait_arrival(near_x.at[j], near_recv.at[j, 0])
+        total = summed[j, 0, parity, 1 - row].astype(jnp.float32) + near_x[j, 1 - row].astype(jnp.float32)
+        passed[j, 0] = total.astype(jnp.bfloat16)
+        send(passed.at[j, 0], far_y.at[j], far_send.at[j, 0], far_recv.at[j, 0], y_side)
+
+    def fold_y(j):
+        wait_arrival(near_y.at[j], near_recv.at[j, 1])
+        total = summed[j, 1, 1 - parity, row].astype(jnp.float32) + near_y[j, 1 - parity].astype(jnp.float32)
+        passed[j, 1] = total.astype(jnp.bfloat16)
+        send(passed.at[j, 1], far_x.at[j], far_send.at[j, 1], far_recv.at[j, 1], x_side)
+
+    def reduce_far(j):
+        wait_arrival(far_y.at[j], far_recv.at[j, 0])
+        wait_arrival(far_x.at[j], far_recv.at[j, 1])
+        left = summed[j, 0, parity, row].astype(jnp.float32) + near_x[j, row].astype(jnp.float32)
+        left = (left + far_y[j].astype(jnp.float32)).astype(jnp.bfloat16)
+        right = summed[j, 1, parity, row].astype(jnp.float32) + near_y[j, parity].astype(jnp.float32)
+        right = (right + far_x[j].astype(jnp.float32)).astype(jnp.bfloat16)
+        if j == 0:
+            out_back[expert, :, :half] = left
+            out_back[expert, :, half:] = right
+            return
+        final[j, :, :half] = left
+        final[j, :, half:] = right
+        target = flipped(expert, j)
+        send(final.at[j], out_back.at[expert], back_send.at[j], back_recv.at[j], (2 * target + parity, tp))
+
+    def weight_grad(n):
+        out, left, right = (
+            (out_down, act, rows_g), (out_gate, dgt, rows_x), (out_up, dup, rows_x)
+        )[n // 4]
+        tile = model_width // 4
+        cols = slice(n % 4 * tile, (n % 4 + 1) * tile)
+        lhs = left[...].reshape(-1, left.shape[-1])
+        rhs = right[:, :, :, cols].reshape(-1, tile)
+        out[:, cols] = dot(lhs, rhs, 0, 0).astype(jnp.bfloat16)
+
+    def share_branch():
+        block = out_b.at[parity, expert]
+        for j in PLAN_CHUNKS:
+            send(block, block, b_send.at[j], b_recv.at[j], (2 * flipped(expert, j) + parity, tp))
+        send(gate_b.at[pl.ds(0, halo)], out_head, h_send.at[0], h_recv.at[0], (before, tp))
+
+    stages = {
+        "depart": depart, "cross": cross, "own": own_stage, "across": across_stage,
+        "near_x": near_x_stage, "near_y": near_y_stage, "far": far_stage,
+        "pre": pre_stage, "hidden": hidden_stage, "back": backward, "pair": reduce_pair,
+        "fold_x": fold_x, "fold_y": fold_y, "home": reduce_far, "grad": weight_grad,
+    }
+    waiting = list(loads)
+    owns = [n for n, stage in enumerate(PLAN) if stage[0] == "own"]
+    for n, (name, *numbers) in enumerate(PLAN):
+        stages[name](*numbers)
+        if n == owns[-1]:
+            share_branch()
+
+    def block_columns(h, line, side_core):
+        return columns(4 * h + 2 * side_core + line, half)
+
+    for j in PLAN_CHUNKS:
+        wait_arrival(out_b.at[parity, flipped(expert, j)], b_recv.at[j])
+    send(out_b.at[parity], out_b.at[parity], b_send.at[0], b_recv.at[0], x_side)
+    for j in PLAN_CHUNKS:
+        wait_arrival(out_back.at[flipped(expert, j)], back_recv.at[j])
+    one_hot = chosen_ref[...].reshape(experts * capacity, tokens)
+    total = dot(one_hot, out_back[...].reshape(experts * capacity, width), 0, 0)
+    guarded = []
+    for h in range(2):
+        cols = block_columns(h, row, core)
+        base = token_g[:, cols].astype(jnp.float32)
+        value = (base + total[:, h * half : (h + 1) * half]).astype(jnp.bfloat16)
+        part_ref[h] = value
+        stream_ref[pl.ds(0, tokens), cols] = value
+    for h in range(2):
+        src, dst, recv = part_ref.at[h], block_ref.at[parity, expert], place_recv.at[parity]
+        away = jnp.logical_or(targets[h][0] != sp, targets[h][1] != tp)
+        copy = pltpu.make_async_remote_copy(
+            src_ref=src, dst_ref=dst, send_sem=place_send.at[h], recv_sem=recv,
+            device_id=targets[h], device_id_type=MESH,
+        )
+
+        @pl.when(away)
+        def _(copy=copy):
+            copy.start()
+
+        @pl.when(jnp.logical_not(away))
+        def _(src=src, dst=dst, recv=recv):
+            pltpu.make_async_copy(src, dst, recv).start()
+
+        guarded.append((away, copy))
+        cols = block_columns(h, row, core)
+        dst = stream_ref.at[pl.ds(0, tokens), cols]
+        send(src, dst, gather_send.at[h, 0], gather_recv.at[h, 0], y_side)
+        send(src, dst, gather_send.at[h, 1], gather_recv.at[h, 1], pair)
+        for n in range(n_tp):
+            send(src.at[pl.ds(0, halo)], stream_ref.at[pl.ds(tokens, halo), cols],
+                 halo_send.at[h, n], halo_recv.at[h, n], (before, lax.rem(tp + n, n_tp)))
+    for h in range(2):
+        block = stream_ref.at[pl.ds(0, tokens), block_columns(h, 1 - row, core)]
+        wait_arrival(block, gather_recv.at[h, 0])
+        send(block, block, gather_send.at[h, 2], gather_recv.at[h, 2], pair)
+    for par in range(2):
+        block = block_ref.at[par, tp]
+        wait_arrival(block, place_recv.at[par])
+        send(block, block, held_send.at[par, 0], held_recv.at[par, 0], y_side)
+        send(block, block, held_send.at[par, 1], held_recv.at[par, 1], pair)
+    for par in range(2):
+        block = block_ref.at[par, other_quarter]
+        wait_arrival(block, held_recv.at[par, 0])
+        send(block, block, held_send.at[par, 2], held_recv.at[par, 2], pair)
+    wait_arrival(out_b.at[1 - parity], b_recv.at[0])
+    wait_arrival(out_head, h_recv.at[0])
+    for h in range(2):
+        for line, slot in ((row, 1), (1 - row, 2)):
+            wait_arrival(
+                stream_ref.at[pl.ds(0, tokens), block_columns(h, line, 1 - core)], gather_recv.at[h, slot]
+            )
+        for n in range(n_tp):
+            source = lax.rem(tp + n_tp - n, n_tp)
+            cols = block_columns(h, source // 2, lax.rem(source, 2))
+            wait_arrival(stream_ref.at[pl.ds(tokens, halo), cols], halo_recv.at[h, n])
+    for par in range(2):
+        for line, slot in ((row, 1), (1 - row, 2)):
+            wait_arrival(block_ref.at[par, 2 * line + 1 - core], held_recv.at[par, slot])
+    for copy in started:
+        copy.wait_send()
+    for away, copy in guarded:
+        pl.when(away)(copy.wait_send)
+
+
+def run_experts(
+    chosen, weight_of, token_x, token_g, gate_b, conv_out, wg, wu, wd, halo, n_sp, n_tp
+):
+    experts, capacity, tokens = chosen.shape
+    model_width = token_x.shape[1]
+    width = model_width // n_tp
+    units = wg.shape[0]
+    half = width // 2
+    channels = gate_b.shape[1]
+    dma = pltpu.SemaphoreType.DMA
+    bf16 = jnp.bfloat16
+
+    def vmem(*shape):
+        return pltpu.VMEM(shape, bf16)
+
+    rows = vmem(experts, 2, capacity, model_width)
+    hidden = vmem(experts, 2 * capacity, units)
+    blocks = vmem(experts, 2, 2, 2, capacity, half)
+    near = vmem(experts, 2, capacity, half)
+    far = vmem(experts, capacity, half)
+    routed = vmem(experts, capacity, width)
+    weight = vmem(units, model_width)
+    pre = pltpu.VMEM((experts, 2 * capacity, units), jnp.float32)
+    return pl.pallas_call(
+        functools.partial(expert_kernel, n_sp, n_tp),
+        out_shape=(
+            vmem(tokens + halo, model_width), vmem(2, experts, tokens, half),
+            vmem(2, experts, tokens, channels), vmem(halo, channels),
+            weight, weight, weight,
+        ),
+        in_specs=[VMEM] * 6 + [ANY] * 3,
+        out_specs=(VMEM,) * 7,
+        scratch_shapes=[
+            routed, routed, routed, vmem(2, tokens, half),
+            rows, rows, hidden, hidden, hidden, blocks, blocks, blocks, blocks,
+            near, near, near, far, far, routed,
+            weight, weight, weight, pre, pre,
+            dma((3,)), dma((2, experts)), dma((2, experts)), dma((2, 2)), dma((2, 2)),
+            dma((2, experts, 2)), dma((2, experts, 2)), dma((2, experts)), dma((2, experts)),
+            dma((2, experts, 4)), dma((2, experts, 4)), dma((2, 2)), dma((2, 2)),
+            dma((experts,)), dma((experts,)), dma((1,)), dma((1,)),
+            dma((experts,)), dma((experts,)), dma((experts, 2)), dma((experts, 2)),
+            dma((experts, 2)), dma((experts, 2)), dma((experts,)), dma((experts,)),
+            dma((2, 3)), dma((2, 3)), dma((2, n_tp)), dma((2, n_tp)),
+            dma((2,)), dma((2,)), dma((2, 3)), dma((2, 3)),
+        ],
+        compiler_params=pltpu.CompilerParams(
+            collective_id=3, has_side_effects=True, vmem_limit_bytes=48 * 1024 * 1024
+        ),
+    )(chosen, weight_of, token_x, token_g, gate_b, conv_out, wg, wu, wd)
+
+
+def tail_kernel(
+    n_sp, stream, blocks, branches, next_gate, out_proj, conv_out, gate_b, gate_c, hidden_h, taps,
+    grad_gate, grad_up, grad_down,
+    out_gate, out_up, out_down, out_p, out_hidden, out_gate_b, out_gate_c,
+    extended, sems,
+):
+    tokens, channels = conv_out.shape
+    moves = [
+        pltpu.make_async_copy(src, dst, sems.at[n])
+        for n, (src, dst) in enumerate(
+            ((grad_gate, out_gate), (grad_up, out_up), (grad_down, out_down))
+        )
+    ]
+    for move in moves:
+        move.start()
+    reach = taps.shape[0] - 1
+    d_branch = dot(stream[...], out_proj[...], 1, 0)
+    last = lax.axis_index("sp") == n_sp - 1
+    following = jnp.where(last, 0.0, d_branch[tokens:] * next_gate[...].astype(jnp.float32))
+    d_branch = d_branch[:tokens]
+    out_gate_b[...] = (d_branch * conv_out[...].astype(jnp.float32)).astype(jnp.bfloat16)
+    extended[pl.ds(0, tokens)] = d_branch * gate_b[...].astype(jnp.float32)
+    extended[pl.ds(tokens, next_gate.shape[0])] = following
+    d_input = jnp.zeros((tokens, channels), jnp.float32)
+    for tap in range(reach + 1):
+        d_input = d_input + taps[tap : tap + 1] * extended[pl.ds(reach - tap, tokens)]
+    out_hidden[...] = (d_input * gate_c[...].astype(jnp.float32)).astype(jnp.bfloat16)
+    out_gate_c[...] = (d_input * hidden_h[...].astype(jnp.float32)).astype(jnp.bfloat16)
+    out_p[...] = dot(
+        blocks[...].reshape(-1, blocks.shape[-1]), branches[...].reshape(-1, channels), 0, 0
+    )
+    for move in moves:
+        move.wait()
+
+
+def run_tail(stream, blocks, branches, next_gate, out_proj, conv_out, gate_b, gate_c, hidden_h, taps, grads, n_sp):
+    tokens, channels = conv_out.shape
+    halo = next_gate.shape[0]
+    small = jax.ShapeDtypeStruct((tokens, channels), jnp.bfloat16)
+    grad = jax.ShapeDtypeStruct(grads[0].shape, jnp.bfloat16)
+    return pl.pallas_call(
+        functools.partial(tail_kernel, n_sp),
+        out_shape=(
+            grad, grad, grad,
+            jax.ShapeDtypeStruct((blocks.shape[-1], channels), jnp.float32), small, small, small,
+        ),
+        in_specs=[VMEM] * 13,
+        out_specs=(ANY,) * 3 + (VMEM,) * 4,
+        scratch_shapes=[
+            pltpu.VMEM((tokens + halo, channels), jnp.float32), pltpu.SemaphoreType.DMA((3,)),
+        ],
+        compiler_params=pltpu.CompilerParams(vmem_limit_bytes=24 * 1024 * 1024),
+    )(stream, blocks, branches, next_gate, out_proj, conv_out, gate_b, gate_c, hidden_h, taps, *grads)
+
+
 def stream_kernel(
     n_sp, n_tp, part_ref, stream_ref, block_ref,
     tp_send, tp_recv, h_send, h_recv, b_send, b_recv, s_send, s_recv,
@@ -447,6 +899,22 @@
     slots = jnp.arange(slot_count, dtype=jnp.int32)
     hits = slots[:, None, None] == positions[None]
     chosen = jnp.any(hits, axis=2).astype(jnp.bfloat16)
+    halo = 16
+    aligned = model_width % (seq_devices * 128) == 0
+    planned = aligned and experts == len(PLAN_CHUNKS) + 1 and n_tp == experts
+    if planned:
+        weight_of = jnp.sum(jnp.where(hits, route_weights[None], 0.0), axis=2)
+        stream, blocks, branches, next_gate, *grads = run_experts(
+            chosen.reshape(experts, capacity, tokens_here),
+            weight_of.reshape(experts, capacity, tokens_here),
+            moe_input, out_grad, gate_b, conv_out, gate_cols.T, up_cols.T, down_rows,
+            halo, seq_devices, n_tp,
+        )
+        grad_gate, grad_up, *rest = run_tail(
+            stream, blocks, branches, next_gate, out_proj, conv_out, gate_b, gate_c, hidden_h,
+            conv_taps, grads, seq_devices,
+        )
+        return (grad_gate.T, grad_up.T, *rest[:2], rest[2], rest[3], rest[4])
     slot_weight = jnp.sum(jnp.where(hits, route_weights[None], 0.0), axis=(1, 2))
     quarter = model_width // n_tp
     column_start = lax.axis_index("tp") * quarter
@@ -456,7 +924,6 @@
     sent_g = jnp.dot(chosen, source_g, preferred_element_type=jnp.float32)
     sent_g = (slot_weight[:, None] * sent_g).astype(jnp.bfloat16)
     branch = (gate_b.astype(jnp.float32) * conv_out.astype(jnp.float32)).astype(jnp.bfloat16)
-    halo = 16
     rows_x, rows_g, all_branch, next_gate_b = dispatch(
         sent_x.reshape(experts, capacity, quarter),
         sent_g.reshape(experts, capacity, quarter),
@@ -489,7 +956,6 @@
     stream_part = (source_g.astype(jnp.float32) + contract_rows(chosen, returned)).astype(
         jnp.bfloat16
     )
-    aligned = model_width % (seq_devices * 128) == 0
     if aligned:
         stream, stream_block = share_stream(stream_part, halo, seq_devices, n_tp)
         grad_proj = contract_rows(

time: 126 us -> 82.2 us (0.65)
  matrix products: 25.5 us -> 0.2 us
  Pallas kernels: 92 us -> 77 us
  local copies, waits for them, and re-layouts: 2.79 us -> 1.14 us
  other arithmetic: 4.29 us -> 2.84 us
    dot_general x13 -> x0, matrix products: 25.3 us -> none  [the longest x5 12.4 us: contract_rows(): lax.dot_general(left_side, right_side, (((0,), (0,)), ((), ())), preferre...]
    pallas_call x3 -> x2, Pallas kernels: 92 us -> 77 us  [the longest x1 73.6 us: run_experts(): pl.pallas_call(functools.partial(expert_kernel, n_sp, n_tp), out_shape=(v...]
    convert_element_type x4 -> x1, other arithmetic: 2.7 us -> 0.66 us  [per_device(): chosen = jnp.any(hits, axis=2).astype(jnp.bfloat16)]
where the time goes in v2:
time: 82.2 us; the launch traced here: 82 us
  Pallas kernels  77 us (94%)
  other arithmetic  2.84 us (3%)
  local copies, waits for them, and re-layouts  1.14 us (1%)
  between operations  0.89 us (1%)
    pallas_call x1, Pallas kernels, run_experts(): pl.pallas_call(functools.partial(expert_kernel, n_sp, n_tp), out_shape=(v...  73.6 us
    pallas_call x1, Pallas kernels, run_tail(): pl.pallas_call(functools.partial(tail_kernel, n_sp), out_shape=(grad, gra...  3.35 us

profile of v2, /device:TPU:0, one launch (start us, length us, event | category | flops | bytes accessed | tf_op | source)
XLA Modules:
  0.0 82.0 jit_solution(10939015635294086295)
XLA Ops:
  0.6 0.8 copy.30
  1.4 0.1 eq.29
  1.6 0.2 fusion
  1.8 0.1 convert_element_type.18
  1.9 0.1 copy.31
  2.0 0.7 multiply_add_fusion
  2.7 0.7 convert_element_type.21
  3.4 1.4 %select_reduce_fusion = f32[384,128]{1,0:T(8,128)} fusion(f32[128,2]{0,1:T(2,128)} %param.16, s32[128,2]{0,1:T(2,128)S(1)} %multiply_add_fusion), kind=kLoop, calls=%fused_computation.2 | loop fusion | flops 245760 | bytes 198656 | tf_op jit(solution)/shard_map/reduce_sum | solution.py:906
  4.8 0.0 copy-start
  4.8 0.0 copy-start.1
  4.8 0.0 copy-start.2
  4.8 0.0 copy-start.3
  4.8 0.0 copy-start.4
  4.8 0.0 copy-start.5
  4.8 73.6 %shard_map.180 = (bf16[144,2048]{1,0:T(8,128)(2,1)S(1)}, bf16[2,4,128,256]{3,2,1,0:T(8,128)(2,1)S(1)}, bf16[2,4,128,128]{3,2,1,0:T(8,128)(2,1)S(1)}, bf16[16,128...) custom-call(bf16[4,96,128]{2,1,0:T(8,128)(2,1)} %bitcast.9, ...), custom_call_target="tpu_custom_call" | custom-call | tf_op jit(solution)/shard_map/pallas_call | solution.py:675
  78.5 0.0 copy-done
  78.5 0.0 copy-done.1
  78.5 0.0 copy-done.2
  78.5 0.0 copy-done.3
  78.5 0.0 copy-done.4
  78.5 0.0 copy-done.5
  78.5 3.4 %shard_map.181 = (bf16[448,2048]{1,0:T(8,128)(2,1)}, bf16[448,2048]{1,0:T(8,128)(2,1)}, bf16[448,2048]{1,0:T(8,128)(2,1)}, f32[256,128]{1,0:T(8,128)}, bf16[128,...) custom-call(bf16[144,2048]{1,0:T(8,128)(2,1)S(1)} %get-tuple-element.21.stream, ...), custom_call_target="tpu_custom_call" | custom-call | tf_op jit(solution)/shard_map/pallas_call | solution.py:744
  (2 shorter events, 0.1 us)
Async XLA Ops:
  4.8 73.6 %copy-start = (bf16[2048,128]{1,0:T(8,128)(2,1)S(1)}, bf16[2048,128]{1,0:T(8,128)(2,1)}, u32[]{:S(2)}) copy-start(bf16[2048,128]{1,0:T(8,128)(2,1)} %out_proj.1) | copy-start | bytes 1572868
  4.8 73.6 %copy-start.1 = (bf16[128,128]{1,0:T(8,128)(2,1)S(1)}, bf16[128,128]{1,0:T(8,128)(2,1)}, u32[]{:S(2)}) copy-start(bf16[128,128]{1,0:T(8,128)(2,1)} %gate_b.3) | copy-start | bytes 98308
  4.8 73.7 %copy-start.2 = (bf16[128,128]{1,0:T(8,128)(2,1)S(1)}, bf16[128,128]{1,0:T(8,128)(2,1)}, u32[]{:S(2)}) copy-start(bf16[128,128]{1,0:T(8,128)(2,1)} %conv_out.3) | copy-start | bytes 98308
  4.8 73.7 %copy-start.3 = (bf16[128,128]{1,0:T(8,128)(2,1)S(1)}, bf16[128,128]{1,0:T(8,128)(2,1)}, u32[]{:S(2)}) copy-start(bf16[128,128]{1,0:T(8,128)(2,1)} %gate_c.1) | copy-start | bytes 98308
  4.8 73.7 %copy-start.4 = (bf16[128,128]{1,0:T(8,128)(2,1)S(1)}, bf16[128,128]{1,0:T(8,128)(2,1)}, u32[]{:S(2)}) copy-start(bf16[128,128]{1,0:T(8,128)(2,1)} %hidden_h.1) | copy-start | bytes 98308
  4.8 73.7 %copy-start.5 = (f32[3,128]{1,0:T(4,128)S(1)}, f32[3,128]{1,0:T(4,128)}, u32[]{:S(2)}) copy-start(f32[3,128]{1,0:T(4,128)} %taps.1) | copy-start | bytes 4612

commit v3 on v2

--- a/solution.py
+++ b/solution.py
@@ -16,7 +16,7 @@
 
 MESH = pl.DeviceIdType.MESH
 VMEM = pl.BlockSpec(memory_space=pltpu.VMEM)
-ANY = pl.BlockSpec(memory_space=pl.ANY)
+HBM = pl.BlockSpec(memory_space=pltpu.HBM)
 
 
 def columns(index, width):
@@ -339,17 +339,23 @@
 
 
 def expert_kernel(
-    n_sp, n_tp,
-    chosen_ref, weight_ref, token_x, token_g, gate_b, conv_out, gate_ref, up_ref, down_ref,
-    stream_ref, block_ref, out_b, out_head, out_gate, out_up, out_down,
-    sent_x, sent_g, out_back, part_ref,
-    rows_x, rows_g, act, dup, dgt, part_out, part_mine, from_pair, summed,
-    near_x, near_y, passed, far_x, far_y, final, wg, wu, wd, gate_pre, up_pre,
-    w_sem, z_send, z_recv, own_send, own_recv, line_send, line_recv, relay_send, relay_recv,
-    pair_send, pair_recv, own_pair_send, own_pair_recv, b_send, b_recv, h_send, h_recv,
-    rp_send, rp_recv, near_send, near_recv, far_send, far_recv, back_send, back_recv,
-    gather_send, gather_recv, halo_send, halo_recv, place_send, place_recv, held_send, held_recv,
+    n_sp, n_tp, *refs,
 ):
+    hbm, refs = refs[:13], refs[13:]
+    out_gate, out_up, out_down, out_proj_grad, out_hidden, out_gate_b, out_gate_c = refs[:7]
+    vmem, refs = refs[7:20], refs[20:]
+    routes, route_weights, token_x, token_g, gate_b, conv_out, *vmem_rest = vmem
+    gate_c, hidden_h, wg, wu, wd, out_proj, taps = vmem_rest
+    (
+        stream_ref, block_ref, out_b, out_head, chosen_ref, weight_ref, extended,
+        sent_x, sent_g, out_back, part_ref,
+        rows_x, rows_g, act, dup, dgt, part_out, part_mine, from_pair, summed,
+        near_x, near_y, passed, far_x, far_y, final, gate_pre, up_pre,
+        load_sem, z_send, z_recv, own_send, own_recv, line_send, line_recv, relay_send, relay_recv,
+        pair_send, pair_recv, own_pair_send, own_pair_recv, b_send, b_recv, h_send, h_recv,
+        rp_send, rp_recv, near_send, near_recv, far_send, far_recv, back_send, back_recv,
+        gather_send, gather_recv, halo_send, halo_recv, place_send, place_recv, held_send, held_recv,
+    ) = refs
     experts = n_sp // 2
     sp, tp, expert, parity, row, core = place(n_tp)
     capacity, width = sent_x.shape[1:]
@@ -375,8 +381,7 @@
         return rows[t].at[flipped(expert, j), par, :, columns(quarter, width)]
 
     loads = [
-        pltpu.make_async_copy(src, dst, w_sem.at[n])
-        for n, (src, dst) in enumerate(((gate_ref, wg), (up_ref, wu), (down_ref, wd)))
+        pltpu.make_async_copy(src, dst, load_sem.at[n]) for n, (src, dst) in enumerate(zip(hbm, vmem))
     ]
     for load in loads:
         load.start()
@@ -397,6 +402,27 @@
             pl.semaphore_signal(barrier, inc=1, device_id=peer, device_id_type=MESH)
 
         expected = expected + away.astype(jnp.int32)
+    for load in loads[:2]:
+        load.wait()
+    lanes = lax.broadcasted_iota(jnp.int32, (tokens, tokens), 1)
+    below = lax.broadcasted_iota(jnp.int32, (tokens, tokens), 0) < lanes
+    first, second = routes[0:1], routes[1:2]
+    ids = lax.broadcasted_iota(jnp.int32, (16, tokens), 0)
+    first_hot = (ids == first).astype(jnp.float32)
+    count = first_hot + (ids == second).astype(jnp.float32)
+    earlier = dot(count.astype(jnp.bfloat16), below.astype(jnp.bfloat16), 1, 0)
+    slot = lax.broadcasted_iota(jnp.int32, (capacity, tokens), 0)
+    for e in range(experts):
+        rank = earlier[e : e + 1].astype(jnp.int32)
+        again = rank + first_hot[e : e + 1].astype(jnp.int32)
+        hit = slot == jnp.where(first == e, rank, -1)
+        hit_again = slot == jnp.where(second == e, again, -1)
+        chosen_ref[e] = jnp.logical_or(hit, hit_again).astype(jnp.float32).astype(jnp.bfloat16)
+        weight_ref[e] = jnp.where(hit, route_weights[0:1], 0.0) + jnp.where(
+            hit_again, route_weights[1:2], 0.0
+        )
+    for load in loads[2:6]:
+        load.wait()
     out_b[parity, expert] = (
         gate_b[...].astype(jnp.float32) * conv_out[...].astype(jnp.float32)
     ).astype(jnp.bfloat16)
@@ -568,7 +594,7 @@
         "pre": pre_stage, "hidden": hidden_stage, "back": backward, "pair": reduce_pair,
         "fold_x": fold_x, "fold_y": fold_y, "home": reduce_far, "grad": weight_grad,
     }
-    waiting = list(loads)
+    waiting = loads[6:]
     owns = [n for n, stage in enumerate(PLAN) if stage[0] == "own"]
     for n, (name, *numbers) in enumerate(PLAN):
         stages[name](*numbers)
@@ -625,12 +651,6 @@
         wait_arrival(block, place_recv.at[par])
         send(block, block, held_send.at[par, 0], held_recv.at[par, 0], y_side)
         send(block, block, held_send.at[par, 1], held_recv.at[par, 1], pair)
-    for par in range(2):
-        block = block_ref.at[par, other_quarter]
-        wait_arrival(block, held_recv.at[par, 0])
-        send(block, block, held_send.at[par, 2], held_recv.at[par, 2], pair)
-    wait_arrival(out_b.at[1 - parity], b_recv.at[0])
-    wait_arrival(out_head, h_recv.at[0])
     for h in range(2):
         for line, slot in ((row, 1), (1 - row, 2)):
             wait_arrival(
@@ -640,29 +660,53 @@
             source = lax.rem(tp + n_tp - n, n_tp)
             cols = block_columns(h, source // 2, lax.rem(source, 2))
             wait_arrival(stream_ref.at[pl.ds(tokens, halo), cols], halo_recv.at[h, n])
+    wait_arrival(out_head, h_recv.at[0])
+    channels = conv_out.shape[1]
+    reach = taps.shape[0] - 1
+    d_branch = dot(stream_ref[...], out_proj[...], 1, 0)
+    following = jnp.where(sp == n_sp - 1, 0.0, d_branch[tokens:] * out_head[...].astype(jnp.float32))
+    d_branch = d_branch[:tokens]
+    out_gate_b[...] = (d_branch * conv_out[...].astype(jnp.float32)).astype(jnp.bfloat16)
+    extended[pl.ds(0, tokens)] = d_branch * gate_b[...].astype(jnp.float32)
+    extended[pl.ds(tokens, halo)] = following
+    d_input = jnp.zeros((tokens, channels), jnp.float32)
+    for tap in range(reach + 1):
+        d_input = d_input + taps[tap : tap + 1] * extended[pl.ds(reach - tap, tokens)]
+    out_hidden[...] = (d_input * gate_c[...].astype(jnp.float32)).astype(jnp.bfloat16)
+    out_gate_c[...] = (d_input * hidden_h[...].astype(jnp.float32)).astype(jnp.bfloat16)
+    for par in range(2):
+        block = block_ref.at[par, other_quarter]
+        wait_arrival(block, held_recv.at[par, 0])
+        send(block, block, held_send.at[par, 2], held_recv.at[par, 2], pair)
+    wait_arrival(out_b.at[1 - parity], b_recv.at[0])
     for par in range(2):
         for line, slot in ((row, 1), (1 - row, 2)):
             wait_arrival(block_ref.at[par, 2 * line + 1 - core], held_recv.at[par, slot])
+    out_proj_grad[...] = dot(
+        block_ref[...].reshape(-1, half), out_b[...].reshape(-1, channels), 0, 0
+    )
     for copy in started:
         copy.wait_send()
     for away, copy in guarded:
         pl.when(away)(copy.wait_send)
 
 
-def run_experts(
-    chosen, weight_of, token_x, token_g, gate_b, conv_out, wg, wu, wd, halo, n_sp, n_tp
-):
-    experts, capacity, tokens = chosen.shape
-    model_width = token_x.shape[1]
+def run_experts(operands, halo, n_sp):
+    _, _, token_x, token_g, gate_b, _, _, _, wg, *_ = operands
+    tokens, model_width = token_x.shape
+    experts = n_tp = n_sp // 2
+    capacity = 2 * (3 * tokens // n_sp)
     width = model_width // n_tp
     units = wg.shape[0]
     half = width // 2
     channels = gate_b.shape[1]
     dma = pltpu.SemaphoreType.DMA
-    bf16 = jnp.bfloat16
 
     def vmem(*shape):
-        return pltpu.VMEM(shape, bf16)
+        return pltpu.VMEM(shape, jnp.bfloat16)
+
+    def wide(*shape):
+        return pltpu.VMEM(shape, jnp.float32)
 
     rows = vmem(experts, 2, capacity, model_width)
     hidden = vmem(experts, 2 * capacity, units)
@@ -671,22 +715,23 @@
     far = vmem(experts, capacity, half)
     routed = vmem(experts, capacity, width)
     weight = vmem(units, model_width)
-    pre = pltpu.VMEM((experts, 2 * capacity, units), jnp.float32)
+    pre = wide(experts, 2 * capacity, units)
+    small = vmem(tokens, channels)
     return pl.pallas_call(
         functools.partial(expert_kernel, n_sp, n_tp),
-        out_shape=(
+        out_shape=(weight, weight, weight, wide(half, channels), small, small, small),
+        in_specs=[HBM] * len(operands),
+        out_specs=(VMEM,) * 7,
+        scratch_shapes=[
+            *(pltpu.VMEM(operand.shape, operand.dtype) for operand in operands),
             vmem(tokens + halo, model_width), vmem(2, experts, tokens, half),
             vmem(2, experts, tokens, channels), vmem(halo, channels),
-            weight, weight, weight,
-        ),
-        in_specs=[VMEM] * 6 + [ANY] * 3,
-        out_specs=(VMEM,) * 7,
-        scratch_shapes=[
+            vmem(experts, capacity, tokens), wide(experts, capacity, tokens),
+            wide(tokens + halo, channels),
             routed, routed, routed, vmem(2, tokens, half),
             rows, rows, hidden, hidden, hidden, blocks, blocks, blocks, blocks,
-            near, near, near, far, far, routed,
-            weight, weight, weight, pre, pre,
-            dma((3,)), dma((2, experts)), dma((2, experts)), dma((2, 2)), dma((2, 2)),
+            near, near, near, far, far, routed, pre, pre,
+            dma((len(operands),)), dma((2, experts)), dma((2, experts)), dma((2, 2)), dma((2, 2)),
             dma((2, experts, 2)), dma((2, experts, 2)), dma((2, experts)), dma((2, experts)),
             dma((2, experts, 4)), dma((2, experts, 4)), dma((2, 2)), dma((2, 2)),
             dma((experts,)), dma((experts,)), dma((1,)), dma((1,)),
@@ -698,62 +743,29 @@
         compiler_params=pltpu.CompilerParams(
             collective_id=3, has_side_effects=True, vmem_limit_bytes=48 * 1024 * 1024
         ),
-    )(chosen, weight_of, token_x, token_g, gate_b, conv_out, wg, wu, wd)
-
-
-def tail_kernel(
-    n_sp, stream, blocks, branches, next_gate, out_proj, conv_out, gate_b, gate_c, hidden_h, taps,
-    grad_gate, grad_up, grad_down,
-    out_gate, out_up, out_down, out_p, out_hidden, out_gate_b, out_gate_c,
-    extended, sems,
-):
-    tokens, channels = conv_out.shape
+    )(*operands)
+
+
+def store_kernel(*refs):
+    count = len(refs) // 2
     moves = [
-        pltpu.make_async_copy(src, dst, sems.at[n])
-        for n, (src, dst) in enumerate(
-            ((grad_gate, out_gate), (grad_up, out_up), (grad_down, out_down))
-        )
+        pltpu.make_async_copy(refs[n], refs[count + n], refs[-1].at[n]) for n in range(count)
     ]
     for move in moves:
         move.start()
-    reach = taps.shape[0] - 1
-    d_branch = dot(stream[...], out_proj[...], 1, 0)
-    last = lax.axis_index("sp") == n_sp - 1
-    following = jnp.where(last, 0.0, d_branch[tokens:] * next_gate[...].astype(jnp.float32))
-    d_branch = d_branch[:tokens]
-    out_gate_b[...] = (d_branch * conv_out[...].astype(jnp.float32)).astype(jnp.bfloat16)
-    extended[pl.ds(0, tokens)] = d_branch * gate_b[...].astype(jnp.float32)
-    extended[pl.ds(tokens, next_gate.shape[0])] = following
-    d_input = jnp.zeros((tokens, channels), jnp.float32)
-    for tap in range(reach + 1):
-        d_input = d_input + taps[tap : tap + 1] * extended[pl.ds(reach - tap, tokens)]
-    out_hidden[...] = (d_input * gate_c[...].astype(jnp.float32)).astype(jnp.bfloat16)
-    out_gate_c[...] = (d_input * hidden_h[...].astype(jnp.float32)).astype(jnp.bfloat16)
-    out_p[...] = dot(
-        blocks[...].reshape(-1, blocks.shape[-1]), branches[...].reshape(-1, channels), 0, 0
-    )
     for move in moves:
         move.wait()
 
 
-def run_tail(stream, blocks, branches, next_gate, out_proj, conv_out, gate_b, gate_c, hidden_h, taps, grads, n_sp):
-    tokens, channels = conv_out.shape
-    halo = next_gate.shape[0]
-    small = jax.ShapeDtypeStruct((tokens, channels), jnp.bfloat16)
-    grad = jax.ShapeDtypeStruct(grads[0].shape, jnp.bfloat16)
+def store(arrays):
     return pl.pallas_call(
-        functools.partial(tail_kernel, n_sp),
-        out_shape=(
-            grad, grad, grad,
-            jax.ShapeDtypeStruct((blocks.shape[-1], channels), jnp.float32), small, small, small,
-        ),
-        in_specs=[VMEM] * 13,
-        out_specs=(ANY,) * 3 + (VMEM,) * 4,
-        scratch_shapes=[
-            pltpu.VMEM((tokens + halo, channels), jnp.float32), pltpu.SemaphoreType.DMA((3,)),
-        ],
-        compiler_params=pltpu.CompilerParams(vmem_limit_bytes=24 * 1024 * 1024),
-    )(stream, blocks, branches, next_gate, out_proj, conv_out, gate_b, gate_c, hidden_h, taps, *grads)
+        store_kernel,
+        out_shape=tuple(jax.ShapeDtypeStruct(a.shape, a.dtype) for a in arrays),
+        in_specs=[VMEM] * len(arrays),
+        out_specs=(HBM,) * len(arrays),
+        scratch_shapes=[pltpu.SemaphoreType.DMA((len(arrays),))],
+        compiler_params=pltpu.CompilerParams(vmem_limit_bytes=16 * 1024 * 1024),
+    )(*arrays)
 
 
 def stream_kernel(
@@ -895,26 +907,22 @@
     capacity = 2 * half_cap
     slot_count = experts * capacity
     n_tp = lax.axis_size("tp")
+    halo = 16
+    aligned = model_width % (seq_devices * 128) == 0
+    planned = aligned and experts == len(PLAN_CHUNKS) + 1 and n_tp == experts
+    if planned and top_count == 2 and conv_taps.shape[0] <= halo:
+        operands = (
+            routes.T, route_weights.T, moe_input, out_grad, gate_b, conv_out, gate_c, hidden_h,
+            gate_cols.T, up_cols.T, down_rows, out_proj, conv_taps,
+        )
+        operands = tuple(pltpu.with_memory_space_constraint(a, pltpu.HBM) for a in operands)
+        grads = run_experts(operands, halo, seq_devices)
+        grad_gate, grad_up, *rest = store(grads)
+        return (grad_gate.T, grad_up.T, *rest)
     positions = slot_choice(routes, experts, capacity)
     slots = jnp.arange(slot_count, dtype=jnp.int32)
     hits = slots[:, None, None] == positions[None]
     chosen = jnp.any(hits, axis=2).astype(jnp.bfloat16)
-    halo = 16
-    aligned = model_width % (seq_devices * 128) == 0
-    planned = aligned and experts == len(PLAN_CHUNKS) + 1 and n_tp == experts
-    if planned:
-        weight_of = jnp.sum(jnp.where(hits, route_weights[None], 0.0), axis=2)
-        stream, blocks, branches, next_gate, *grads = run_experts(
-            chosen.reshape(experts, capacity, tokens_here),
-            weight_of.reshape(experts, capacity, tokens_here),
-            moe_input, out_grad, gate_b, conv_out, gate_cols.T, up_cols.T, down_rows,
-            halo, seq_devices, n_tp,
-        )
-        grad_gate, grad_up, *rest = run_tail(
-            stream, blocks, branches, next_gate, out_proj, conv_out, gate_b, gate_c, hidden_h,
-            conv_taps, grads, seq_devices,
-        )
-        return (grad_gate.T, grad_up.T, *rest[:2], rest[2], rest[3], rest[4])
     slot_weight = jnp.sum(jnp.where(hits, route_weights[None], 0.0), axis=(1, 2))
     quarter = model_width // n_tp
     column_start = lax.axis_index("tp") * quarter

time: 82.2 us -> 75.9 us (0.923)
  other arithmetic: 2.84 us -> 0 us
  Pallas kernels: 77 us -> 74.6 us
  local copies, waits for them, and re-layouts: 1.14 us -> 0 us
    pallas_call x2, Pallas kernels: 77 us -> 74.6 us  [the longest x1 72 us: run_experts(): pl.pallas_call(functools.partial(expert_kernel, n_sp, n_tp), out_shape=(w...]
    reduce_sum x1 -> x0, other arithmetic: 1.42 us -> none  [per_device(): weight_of = jnp.sum(jnp.where(hits, route_weights[None], 0.0), axis=2)]
where the time goes in v3:
time: 75.9 us; the launch traced here: 75.4 us
  Pallas kernels  74.6 us (98%)
  between operations  0.81 us (1%)
    pallas_call x1, Pallas kernels, run_experts(): pl.pallas_call(functools.partial(expert_kernel, n_sp, n_tp), out_shape=(w...  72 us
    pallas_call x1, Pallas kernels, store(): pl.pallas_call(store_kernel, out_shape=tuple((jax.ShapeDtypeStruct(a.shap...  2.55 us

profile of v3, /device:TPU:0, one launch (start us, length us, event | category | flops | bytes accessed | tf_op | source)
XLA Modules:
  0.0 75.4 jit_solution(4838679101684531663)
XLA Ops:
  0.6 72.0 %shard_map.180 = (bf16[448,2048]{1,0:T(8,128)(2,1)S(1)}, bf16[448,2048]{1,0:T(8,128)(2,1)S(1)}, bf16[448,2048]{1,0:T(8,128)(2,1)S(1)}, f32[256,128]{1,0:T(8,128)...) custom-call(s32[2,128]{1,0:T(2,128)} %bitcast.8, ...), custom_call_target="tpu_custom_call" | custom-call | tf_op jit(solution)/shard_map/pallas_call | solution.py:720
  72.7 2.5 %shard_map.181 = (bf16[448,2048]{1,0:T(8,128)(2,1)}, bf16[448,2048]{1,0:T(8,128)(2,1)}, bf16[448,2048]{1,0:T(8,128)(2,1)}, f32[256,128]{1,0:T(8,128)}, bf16[128,...) custom-call(bf16[448,2048]{1,0:T(8,128)(2,1)S(1)} %get-tuple-element.21.refs_0_, ...), custom_call_target="tpu_custom_call" | custom-call | tf_op jit(solution)/shard_map/pallas_call | solution.py:761

commit v4 on v3

--- a/solution.py
+++ b/solution.py
@@ -321,20 +321,22 @@
 
 
 PLAN_CHUNKS = (1, 3, 2)
-PLAN_OVER_X = (0, 4,)
+PLAN_OVER_X = (2, 4)
+PLAN_EXTRA = (0, 1)
+PLAN_RELAYED = (0, 1)
 PLAN = (
-    ("depart", 1), ("cross", 0, 1), ("cross", 0, 0), ("depart", 2), ("own", 1), ("cross", 1, 1),
-    ("depart", 0), ("depart", 3), ("own", 0), ("across", 0, 0), ("depart", 4), ("own", 2), ("near_y", 0),
-    ("near_x", 1), ("near_x", 0), ("own", 3), ("across", 0, 1), ("depart", 5), ("near_y", 1),
-    ("across", 1, 1), ("far", 1), ("near_x", 2), ("far", 0), ("own", 4), ("pre", 1), ("near_y", 2),
-    ("near_x", 3), ("hidden", 1), ("far", 2), ("own", 5), ("pre", 0), ("near_x", 4), ("back", 1),
-    ("near_y", 4), ("pre", 3), ("near_y", 3), ("cross", 1, 0), ("far", 3), ("near_x", 5), ("pair", 1),
-    ("hidden", 3), ("far", 4), ("back", 3), ("pre", 2), ("near_y", 5), ("far", 5), ("pair", 3), ("hidden", 2),
-    ("fold_x", 1), ("across", 1, 0), ("fold_y", 1), ("back", 2), ("fold_x", 3), ("fold_y", 3), ("pair", 2),
-    ("home", 1), ("hidden", 0), ("back", 0), ("home", 3), ("fold_y", 2), ("fold_x", 2), ("grad", 6),
-    ("pair", 0), ("grad", 5), ("grad", 8), ("home", 2), ("grad", 2), ("grad", 3), ("grad", 0), ("grad", 9),
-    ("fold_x", 0), ("fold_y", 0), ("grad", 11), ("grad", 7), ("grad", 4), ("grad", 10), ("grad", 1),
-    ("home", 0),
+    ("depart", 3), ("depart", 0), ("cross", 1, 0), ("depart", 2), ("cross", 0, 0), ("depart", 1),
+    ("depart", 4), ("across", 1, 0), ("across", 0, 0), ("own", 3), ("own", 0), ("aside", 0), ("own", 2),
+    ("near_x", 3), ("extra", 0), ("near_y", 3), ("own", 1), ("aside", 1), ("near_x", 0), ("depart", 5),
+    ("pre", 0), ("near_y", 2), ("near_y", 0), ("share",), ("own", 4), ("hidden", 0), ("far", 3),
+    ("near_x", 1), ("near_x", 2), ("own", 5), ("extra", 1), ("far", 2), ("back", 0), ("pre", 3),
+    ("near_y", 4), ("hidden", 3), ("far", 0), ("near_x", 4), ("near_x", 5), ("back", 3), ("pair_x", 0),
+    ("near_y", 1), ("pre", 1), ("far", 4), ("pair_y", 3), ("pair_x", 3), ("near_y", 5), ("far", 1),
+    ("pair_y", 0), ("far", 5), ("pre", 2), ("hidden", 2), ("back", 2), ("hidden", 1), ("fold_x", 3),
+    ("fold_y", 3), ("back", 1), ("pair_y", 2), ("pair_x", 2), ("pair_x", 1), ("grad", 11), ("grad", 6),
+    ("pair_y", 1), ("home", 3), ("fold_y", 2), ("fold_x", 2), ("fold_y", 1), ("fold_x", 1), ("grad", 8),
+    ("grad", 5), ("home", 2), ("grad", 9), ("fold_y", 0), ("grad", 7), ("fold_x", 0), ("grad", 1),
+    ("home", 1), ("grad", 2), ("grad", 0), ("home", 0), ("grad", 10), ("grad", 4), ("grad", 3),
 )
 
 
@@ -348,7 +350,7 @@
     gate_c, hidden_h, wg, wu, wd, out_proj, taps = vmem_rest
     (
         stream_ref, block_ref, out_b, out_head, chosen_ref, weight_ref, extended,
-        sent_x, sent_g, out_back, part_ref,
+        sent_x, sent_g, extra, out_back, part_ref,
         rows_x, rows_g, act, dup, dgt, part_out, part_mine, from_pair, summed,
         near_x, near_y, passed, far_x, far_y, final, gate_pre, up_pre,
         load_sem, z_send, z_recv, own_send, own_recv, line_send, line_recv, relay_send, relay_recv,
@@ -383,7 +385,7 @@
     loads = [
         pltpu.make_async_copy(src, dst, load_sem.at[n]) for n, (src, dst) in enumerate(zip(hbm, vmem))
     ]
-    for load in loads:
+    for load in loads[:6]:
         load.start()
     before, after = lax.rem(sp + n_sp - 1, n_sp), lax.rem(sp + 1, n_sp)
     fixed = [x_side, y_side, pair] + [(2 * flipped(expert, j) + parity, tp) for j in PLAN_CHUNKS]
@@ -423,33 +425,60 @@
         )
     for load in loads[2:6]:
         load.wait()
+    for load in loads[6:]:
+        load.start()
     out_b[parity, expert] = (
         gate_b[...].astype(jnp.float32) * conv_out[...].astype(jnp.float32)
     ).astype(jnp.bfloat16)
-    slot_weight = jnp.sum(weight_ref[...], axis=2, keepdims=True)
-    mine = columns(tp, width)
-    one_hot = chosen_ref[...].reshape(experts * capacity, tokens)
-    sent_x[...] = dot(one_hot, token_x[:, mine], 1, 0).astype(jnp.bfloat16).reshape(sent_x.shape)
-    scaled = slot_weight * dot(one_hot, token_g[:, mine], 1, 0).reshape(sent_g.shape)
-    sent_g[...] = scaled.astype(jnp.bfloat16)
-    one_hot = chosen_ref[expert]
-    slot_weight = jnp.sum(weight_ref[expert], axis=1, keepdims=True)
-    rows_x[expert, parity] = dot(one_hot, token_x[...], 1, 0).astype(jnp.bfloat16)
-    rows_g[expert, parity] = (slot_weight * dot(one_hot, token_g[...], 1, 0)).astype(jnp.bfloat16)
+    tokens_in, prepared = (token_x, token_g), []
+
+    def select(t, one_hot, weight, cols):
+        value = dot(one_hot, tokens_in[t][:, cols], 1, 0)
+        return (weight * value if t else value).astype(jnp.bfloat16)
+
+    def prepare(kind, t):
+        if (kind, t) not in prepared:
+            prepared.append((kind, t))
+            if kind == "own":
+                weight = jnp.sum(weight_ref[expert], axis=1, keepdims=True)
+                rows[t][expert, parity] = select(t, chosen_ref[expert], weight, slice(None))
+            elif kind == "sent":
+                weight = jnp.sum(weight_ref[...].reshape(-1, tokens), axis=1, keepdims=True)
+                one_hot = chosen_ref[...].reshape(-1, tokens)
+                value = select(t, one_hot, weight, columns(tp, width))
+                sources[t][...] = value.reshape(experts, capacity, width)
+            else:
+                target = flipped(expert, 1)
+                weight = jnp.sum(weight_ref[target], axis=1, keepdims=True)
+                extra[t] = select(t, chosen_ref[target], weight, columns(other_quarter, width))
+
+    for t in range(2):
+        prepare("own", t)
+        prepare("sent", t)
+    for n in PLAN_EXTRA:
+        prepare("extra", n % 2)
     pl.semaphore_wait(barrier, expected)
     steps = [(j, t) for j in PLAN_CHUNKS for t in range(2)]
 
     def depart(n):
         j, t = steps[n]
         target = flipped(expert, j)
+        prepare("sent", t)
         send(sources[t].at[target], rows[t].at[expert, parity, :, columns(tp, width)],
              z_send.at[t, j], z_recv.at[t, j], (2 * target + parity, tp))
 
     def piece(t, par, which, part):
         return rows[t].at[expert, par, :, columns(2 * which + part, width)]
 
+    def depart_extra(n):
+        j, t = steps[n]
+        prepare("extra", t)
+        send(extra.at[t], rows[t].at[expert, parity, :, columns(other_quarter, width)],
+             line_send.at[t, j, 1], line_recv.at[t, j, 1], (2 * flipped(expert, j) + parity, tp))
+
     def cross(t, part):
-        block = piece(t, parity, core, part)
+        prepare("own", t)
+        block = piece(t, parity, core, row if t in PLAN_RELAYED else part)
         send(block, block, own_send.at[t, part], own_recv.at[t, part], x_side)
 
     def own_stage(n):
@@ -457,13 +486,21 @@
         block = spot(t, j, parity, tp)
         wait_arrival(block, z_recv.at[t, j])
         send(block, block, line_send.at[t, j, 0], line_recv.at[t, j, 0], x_side)
-        send(block, block, line_send.at[t, j, 1], line_recv.at[t, j, 1], y_side)
+        if n not in PLAN_EXTRA:
+            send(block, block, line_send.at[t, j, 1], line_recv.at[t, j, 1], y_side)
         send(block, block, pair_send.at[t, j, 0], pair_recv.at[t, j, 0], pair)
 
     def across_stage(t, part):
-        block = piece(t, 1 - parity, core, part)
+        block = piece(t, 1 - parity, core, row if t in PLAN_RELAYED else part)
         wait_arrival(block, own_recv.at[t, part])
+        if t in PLAN_RELAYED:
+            send(block, block, own_send.at[t, 1], own_recv.at[t, 1], y_side)
         send(block, block, own_pair_send.at[t, part], own_pair_recv.at[t, part], pair)
+
+    def aside_stage(t):
+        block = piece(t, 1 - parity, core, 1 - row)
+        wait_arrival(block, own_recv.at[t, 1])
+        send(block, block, own_pair_send.at[t, 1], own_pair_recv.at[t, 1], pair)
 
     def near_x_stage(n):
         j, t = steps[n]
@@ -490,7 +527,8 @@
     def arrived(j, t):
         if j == 0:
             for part in range(2):
-                wait_arrival(piece(t, 1 - parity, 1 - core, part), own_pair_recv.at[t, part])
+                which = lax.rem(row + part, 2) if t in PLAN_RELAYED else part
+                wait_arrival(piece(t, 1 - parity, 1 - core, which), own_pair_recv.at[t, part])
             return
         quarters = (2 * row + 1 - core, 2 * (1 - row) + 1 - core)
         spots = ((parity, quarters[0]), (1 - parity, quarters[0]),
@@ -534,14 +572,20 @@
                     piece = value[par * capacity : (par + 1) * capacity]
                     store[j, h, par, 0] = piece[:, :half]
                     store[j, h, par, 1] = piece[:, half:]
-            if not kept:
-                send(part_out.at[j], from_pair.at[j], rp_send.at[j], rp_recv.at[j], pair)
-
-    def reduce_pair(j):
-        wait_arrival(from_pair.at[j], rp_recv.at[j])
-        total = part_mine[j].astype(jnp.float32) + from_pair[j].astype(jnp.float32)
-        summed[j] = total.astype(jnp.bfloat16)
+                if not kept:
+                    send(part_out.at[j, h], from_pair.at[j, h], rp_send.at[j, h], rp_recv.at[j, h], pair)
+
+    def add_pair(j, h):
+        wait_arrival(from_pair.at[j, h], rp_recv.at[j, h])
+        total = part_mine[j, h].astype(jnp.float32) + from_pair[j, h].astype(jnp.float32)
+        summed[j, h] = total.astype(jnp.bfloat16)
+
+    def pair_x(j):
+        add_pair(j, 0)
         send(summed.at[j, 0, 1 - parity], near_x.at[j], near_send.at[j, 0], near_recv.at[j, 0], x_side)
+
+    def pair_y(j):
+        add_pair(j, 1)
         send(summed.at[j, 1, :, 1 - row], near_y.at[j], near_send.at[j, 1], near_recv.at[j, 1], y_side)
 
     def fold_x(j):
@@ -589,17 +633,16 @@
         send(gate_b.at[pl.ds(0, halo)], out_head, h_send.at[0], h_recv.at[0], (before, tp))
 
     stages = {
-        "depart": depart, "cross": cross, "own": own_stage, "across": across_stage,
+        "depart": depart, "extra": depart_extra, "cross": cross, "own": own_stage,
+        "across": across_stage, "aside": aside_stage,
         "near_x": near_x_stage, "near_y": near_y_stage, "far": far_stage,
-        "pre": pre_stage, "hidden": hidden_stage, "back": backward, "pair": reduce_pair,
+        "pre": pre_stage, "hidden": hidden_stage, "back": backward, "pair_x": pair_x, "pair_y": pair_y,
         "fold_x": fold_x, "fold_y": fold_y, "home": reduce_far, "grad": weight_grad,
+        "share": share_branch,
     }
     waiting = loads[6:]
-    owns = [n for n, stage in enumerate(PLAN) if stage[0] == "own"]
-    for n, (name, *numbers) in enumerate(PLAN):
+    for name, *numbers in PLAN:
         stages[name](*numbers)
-        if n == owns[-1]:
-            share_branch()
 
     def block_columns(h, line, side_core):
         return columns(4 * h + 2 * side_core + line, half)
@@ -728,14 +771,14 @@
             vmem(2, experts, tokens, channels), vmem(halo, channels),
             vmem(experts, capacity, tokens), wide(experts, capacity, tokens),
             wide(tokens + halo, channels),
-            routed, routed, routed, vmem(2, tokens, half),
+            routed, routed, vmem(2, capacity, width), routed, vmem(2, tokens, half),
             rows, rows, hidden, hidden, hidden, blocks, blocks, blocks, blocks,
             near, near, near, far, far, routed, pre, pre,
             dma((len(operands),)), dma((2, experts)), dma((2, experts)), dma((2, 2)), dma((2, 2)),
             dma((2, experts, 2)), dma((2, experts, 2)), dma((2, experts)), dma((2, experts)),
             dma((2, experts, 4)), dma((2, experts, 4)), dma((2, 2)), dma((2, 2)),
             dma((experts,)), dma((experts,)), dma((1,)), dma((1,)),
-            dma((experts,)), dma((experts,)), dma((experts, 2)), dma((experts, 2)),
+            dma((experts, 2)), dma((experts, 2)), dma((experts, 2)), dma((experts, 2)),
             dma((experts, 2)), dma((experts, 2)), dma((experts,)), dma((experts,)),
             dma((2, 3)), dma((2, 3)), dma((2, n_tp)), dma((2, n_tp)),
             dma((2,)), dma((2,)), dma((2, 3)), dma((2, 3)),

time: 75.9 us -> 73 us (0.962)
  Pallas kernels: 74.6 us -> 71.7 us
    pallas_call x1, Pallas kernels: 72 us -> 69.2 us  [run_experts(): pl.pallas_call(functools.partial(expert_kernel, n_sp, n_tp), out_shape=(w...]
where the time goes in v4:
time: 73 us; the launch traced here: 72.5 us
  Pallas kernels  71.7 us (98%)
  between operations  0.81 us (1%)
    pallas_call x1, Pallas kernels, run_experts(): pl.pallas_call(functools.partial(expert_kernel, n_sp, n_tp), out_shape=(w...  69.2 us
    pallas_call x1, Pallas kernels, store(): pl.pallas_call(store_kernel, out_shape=tuple((jax.ShapeDtypeStruct(a.shap...  2.55 us

profile of v4, /device:TPU:0, one launch (start us, length us, event | category | flops | bytes accessed | tf_op | source)
XLA Modules:
  0.0 72.5 jit_solution(6593848864448223538)
XLA Ops:
  0.6 69.2 %shard_map.180 = (bf16[448,2048]{1,0:T(8,128)(2,1)S(1)}, bf16[448,2048]{1,0:T(8,128)(2,1)S(1)}, bf16[448,2048]{1,0:T(8,128)(2,1)S(1)}, f32[256,128]{1,0:T(8,128)...) custom-call(s32[2,128]{1,0:T(2,128)} %bitcast.8, ...), custom_call_target="tpu_custom_call" | custom-call | tf_op jit(solution)/shard_map/pallas_call | solution.py:763
  69.8 2.5 %shard_map.181 = (bf16[448,2048]{1,0:T(8,128)(2,1)}, bf16[448,2048]{1,0:T(8,128)(2,1)}, bf16[448,2048]{1,0:T(8,128)(2,1)}, f32[256,128]{1,0:T(8,128)}, bf16[128,...) custom-call(bf16[448,2048]{1,0:T(8,128)(2,1)S(1)} %get-tuple-element.21.refs_0_, ...), custom_call_target="tpu_custom_call" | custom-call | tf_op jit(solution)/shard_map/pallas_call | solution.py:804

commit v5 on v4

--- a/solution.py
+++ b/solution.py
@@ -321,22 +321,23 @@
 
 
 PLAN_CHUNKS = (1, 3, 2)
-PLAN_OVER_X = (2, 4)
+PLAN_OVER_X = (0, 5)
 PLAN_EXTRA = (0, 1)
-PLAN_RELAYED = (0, 1)
 PLAN = (
-    ("depart", 3), ("depart", 0), ("cross", 1, 0), ("depart", 2), ("cross", 0, 0), ("depart", 1),
-    ("depart", 4), ("across", 1, 0), ("across", 0, 0), ("own", 3), ("own", 0), ("aside", 0), ("own", 2),
-    ("near_x", 3), ("extra", 0), ("near_y", 3), ("own", 1), ("aside", 1), ("near_x", 0), ("depart", 5),
-    ("pre", 0), ("near_y", 2), ("near_y", 0), ("share",), ("own", 4), ("hidden", 0), ("far", 3),
-    ("near_x", 1), ("near_x", 2), ("own", 5), ("extra", 1), ("far", 2), ("back", 0), ("pre", 3),
-    ("near_y", 4), ("hidden", 3), ("far", 0), ("near_x", 4), ("near_x", 5), ("back", 3), ("pair_x", 0),
-    ("near_y", 1), ("pre", 1), ("far", 4), ("pair_y", 3), ("pair_x", 3), ("near_y", 5), ("far", 1),
-    ("pair_y", 0), ("far", 5), ("pre", 2), ("hidden", 2), ("back", 2), ("hidden", 1), ("fold_x", 3),
-    ("fold_y", 3), ("back", 1), ("pair_y", 2), ("pair_x", 2), ("pair_x", 1), ("grad", 11), ("grad", 6),
-    ("pair_y", 1), ("home", 3), ("fold_y", 2), ("fold_x", 2), ("fold_y", 1), ("fold_x", 1), ("grad", 8),
-    ("grad", 5), ("home", 2), ("grad", 9), ("fold_y", 0), ("grad", 7), ("fold_x", 0), ("grad", 1),
-    ("home", 1), ("grad", 2), ("grad", 0), ("home", 0), ("grad", 10), ("grad", 4), ("grad", 3),
+    ("depart", 3), ("cross", 0, 0), ("cross", 0, 1), ("cross", 1, 0), ("cross", 1, 1), ("depart", 0),
+    ("depart", 2), ("depart", 1), ("across", 0, 0), ("across", 0, 1), ("across", 1, 0), ("across", 1, 1),
+    ("depart", 4), ("extra", 0), ("depart", 5), ("own", 3), ("own", 0), ("near_x", 3), ("own", 2),
+    ("aside", 0, 0), ("aside", 0, 1), ("near_y", 3), ("own", 1), ("aside", 1, 0), ("aside", 1, 1),
+    ("near_x", 2), ("far", 3), ("extra", 1), ("own", 4), ("share",), ("near_y", 2), ("pre", 0), ("near_y", 0),
+    ("own", 5), ("far", 2), ("hidden", 0), ("near_x", 4), ("back", 0), ("near_y", 4), ("pre", 3),
+    ("near_x", 1), ("near_y", 1), ("far", 0), ("hidden", 3), ("near_y", 5), ("back", 3), ("near_x", 0),
+    ("near_x", 5), ("pair_x", 3), ("far", 4), ("pair_x", 0), ("pair_y", 3), ("pair_y", 0), ("pre", 1),
+    ("far", 5), ("pre", 2), ("far", 1), ("hidden", 2), ("back", 2), ("fold_y", 3), ("fold_x", 3),
+    ("hidden", 1), ("pair_x", 2), ("pair_y", 2), ("back", 1), ("grad", 3), ("pair_x", 1), ("left", 3),
+    ("right", 3), ("pair_y", 1), ("grad", 5), ("grad", 11), ("grad", 8), ("fold_x", 2), ("grad", 10),
+    ("fold_y", 2), ("fold_y", 0), ("fold_x", 1), ("grad", 9), ("fold_y", 1), ("left", 2), ("right", 2),
+    ("fold_x", 0), ("left", 1), ("right", 1), ("grad", 7), ("grad", 2), ("grad", 4), ("left", 0),
+    ("right", 0), ("grad", 0), ("grad", 1), ("grad", 6),
 )
 
 
@@ -467,8 +468,9 @@
         send(sources[t].at[target], rows[t].at[expert, parity, :, columns(tp, width)],
              z_send.at[t, j], z_recv.at[t, j], (2 * target + parity, tp))
 
-    def piece(t, par, which, part):
-        return rows[t].at[expert, par, :, columns(2 * which + part, width)]
+    def piece(t, par, which, line, part):
+        part = pl.ds(part * (capacity // 2), capacity // 2)
+        return rows[t].at[expert, par, part, columns(2 * which + line, width)]
 
     def depart_extra(n):
         j, t = steps[n]
@@ -477,9 +479,8 @@
              line_send.at[t, j, 1], line_recv.at[t, j, 1], (2 * flipped(expert, j) + parity, tp))
 
     def cross(t, part):
-        prepare("own", t)
-        block = piece(t, parity, core, row if t in PLAN_RELAYED else part)
-        send(block, block, own_send.at[t, part], own_recv.at[t, part], x_side)
+        block = piece(t, parity, core, row, part)
+        send(block, block, own_send.at[t, 0, part], own_recv.at[t, 0, part], x_side)
 
     def own_stage(n):
         j, t = steps[n]
@@ -491,16 +492,15 @@
         send(block, block, pair_send.at[t, j, 0], pair_recv.at[t, j, 0], pair)
 
     def across_stage(t, part):
-        block = piece(t, 1 - parity, core, row if t in PLAN_RELAYED else part)
-        wait_arrival(block, own_recv.at[t, part])
-        if t in PLAN_RELAYED:
-            send(block, block, own_send.at[t, 1], own_recv.at[t, 1], y_side)
-        send(block, block, own_pair_send.at[t, part], own_pair_recv.at[t, part], pair)
-
-    def aside_stage(t):
-        block = piece(t, 1 - parity, core, 1 - row)
-        wait_arrival(block, own_recv.at[t, 1])
-        send(block, block, own_pair_send.at[t, 1], own_pair_recv.at[t, 1], pair)
+        block = piece(t, 1 - parity, core, row, part)
+        wait_arrival(block, own_recv.at[t, 0, part])
+        send(block, block, own_send.at[t, 1, part], own_recv.at[t, 1, part], y_side)
+        send(block, block, own_pair_send.at[t, 0, part], own_pair_recv.at[t, 0, part], pair)
+
+    def aside_stage(t, part):
+        block = piece(t, 1 - parity, core, 1 - row, part)
+        wait_arrival(block, own_recv.at[t, 1, part])
+        send(block, block, own_pair_send.at[t, 1, part], own_pair_recv.at[t, 1, part], pair)
 
     def near_x_stage(n):
         j, t = steps[n]
@@ -527,8 +527,9 @@
     def arrived(j, t):
         if j == 0:
             for part in range(2):
-                which = lax.rem(row + part, 2) if t in PLAN_RELAYED else part
-                wait_arrival(piece(t, 1 - parity, 1 - core, which), own_pair_recv.at[t, part])
+                for n, line in enumerate((row, 1 - row)):
+                    block = piece(t, 1 - parity, 1 - core, line, part)
+                    wait_arrival(block, own_pair_recv.at[t, n, part])
             return
         quarters = (2 * row + 1 - core, 2 * (1 - row) + 1 - core)
         spots = ((parity, quarters[0]), (1 - parity, quarters[0]),
@@ -600,21 +601,24 @@
         passed[j, 1] = total.astype(jnp.bfloat16)
         send(passed.at[j, 1], far_x.at[j], far_send.at[j, 1], far_recv.at[j, 1], x_side)
 
-    def reduce_far(j):
+    def go_home(j, h, value):
+        cols = pl.ds(h * half, half)
+        if j == 0:
+            out_back[expert, :, cols] = value
+            return
+        final[j, :, cols] = value
+        send(final.at[j, :, cols], out_back.at[expert, :, cols], back_send.at[j, h], back_recv.at[j, h],
+             (2 * flipped(expert, j) + parity, tp))
+
+    def home_left(j):
         wait_arrival(far_y.at[j], far_recv.at[j, 0])
+        total = summed[j, 0, parity, row].astype(jnp.float32) + near_x[j, row].astype(jnp.float32)
+        go_home(j, 0, (total + far_y[j].astype(jnp.float32)).astype(jnp.bfloat16))
+
+    def home_right(j):
         wait_arrival(far_x.at[j], far_recv.at[j, 1])
-        left = summed[j, 0, parity, row].astype(jnp.float32) + near_x[j, row].astype(jnp.float32)
-        left = (left + far_y[j].astype(jnp.float32)).astype(jnp.bfloat16)
-        right = summed[j, 1, parity, row].astype(jnp.float32) + near_y[j, parity].astype(jnp.float32)
-        right = (right + far_x[j].astype(jnp.float32)).astype(jnp.bfloat16)
-        if j == 0:
-            out_back[expert, :, :half] = left
-            out_back[expert, :, half:] = right
-            return
-        final[j, :, :half] = left
-        final[j, :, half:] = right
-        target = flipped(expert, j)
-        send(final.at[j], out_back.at[expert], back_send.at[j], back_recv.at[j], (2 * target + parity, tp))
+        total = summed[j, 1, parity, row].astype(jnp.float32) + near_y[j, parity].astype(jnp.float32)
+        go_home(j, 1, (total + far_x[j].astype(jnp.float32)).astype(jnp.bfloat16))
 
     def weight_grad(n):
         out, left, right = (
@@ -632,26 +636,33 @@
             send(block, block, b_send.at[j], b_recv.at[j], (2 * flipped(expert, j) + parity, tp))
         send(gate_b.at[pl.ds(0, halo)], out_head, h_send.at[0], h_recv.at[0], (before, tp))
 
+    def cross_branch():
+        for j in PLAN_CHUNKS:
+            wait_arrival(out_b.at[parity, flipped(expert, j)], b_recv.at[j])
+        send(out_b.at[parity], out_b.at[parity], b_send.at[0], b_recv.at[0], x_side)
+
     stages = {
         "depart": depart, "extra": depart_extra, "cross": cross, "own": own_stage,
         "across": across_stage, "aside": aside_stage,
         "near_x": near_x_stage, "near_y": near_y_stage, "far": far_stage,
         "pre": pre_stage, "hidden": hidden_stage, "back": backward, "pair_x": pair_x, "pair_y": pair_y,
-        "fold_x": fold_x, "fold_y": fold_y, "home": reduce_far, "grad": weight_grad,
+        "fold_x": fold_x, "fold_y": fold_y, "left": home_left, "right": home_right, "grad": weight_grad,
         "share": share_branch,
     }
     waiting = loads[6:]
-    for name, *numbers in PLAN:
+    folds = [n for n, stage in enumerate(PLAN) if stage[0] in ("fold_x", "fold_y")]
+    for n, (name, *numbers) in enumerate(PLAN):
         stages[name](*numbers)
+        if n == folds[-1]:
+            cross_branch()
 
     def block_columns(h, line, side_core):
         return columns(4 * h + 2 * side_core + line, half)
 
     for j in PLAN_CHUNKS:
-        wait_arrival(out_b.at[parity, flipped(expert, j)], b_recv.at[j])
-    send(out_b.at[parity], out_b.at[parity], b_send.at[0], b_recv.at[0], x_side)
-    for j in PLAN_CHUNKS:
-        wait_arrival(out_back.at[flipped(expert, j)], back_recv.at[j])
+        for h in range(2):
+            block = out_back.at[flipped(expert, j), :, pl.ds(h * half, half)]
+            wait_arrival(block, back_recv.at[j, h])
     one_hot = chosen_ref[...].reshape(experts * capacity, tokens)
     total = dot(one_hot, out_back[...].reshape(experts * capacity, width), 0, 0)
     guarded = []
@@ -678,22 +689,25 @@
             pltpu.make_async_copy(src, dst, recv).start()
 
         guarded.append((away, copy))
-        cols = block_columns(h, row, core)
+    for h in range(2):
+        src, cols = part_ref.at[h], block_columns(h, row, core)
         dst = stream_ref.at[pl.ds(0, tokens), cols]
         send(src, dst, gather_send.at[h, 0], gather_recv.at[h, 0], y_side)
         send(src, dst, gather_send.at[h, 1], gather_recv.at[h, 1], pair)
+    for h in range(2):
+        src, cols = part_ref.at[h], block_columns(h, row, core)
         for n in range(n_tp):
             send(src.at[pl.ds(0, halo)], stream_ref.at[pl.ds(tokens, halo), cols],
                  halo_send.at[h, n], halo_recv.at[h, n], (before, lax.rem(tp + n, n_tp)))
-    for h in range(2):
-        block = stream_ref.at[pl.ds(0, tokens), block_columns(h, 1 - row, core)]
-        wait_arrival(block, gather_recv.at[h, 0])
-        send(block, block, gather_send.at[h, 2], gather_recv.at[h, 2], pair)
     for par in range(2):
         block = block_ref.at[par, tp]
         wait_arrival(block, place_recv.at[par])
         send(block, block, held_send.at[par, 0], held_recv.at[par, 0], y_side)
         send(block, block, held_send.at[par, 1], held_recv.at[par, 1], pair)
+    for h in range(2):
+        block = stream_ref.at[pl.ds(0, tokens), block_columns(h, 1 - row, core)]
+        wait_arrival(block, gather_recv.at[h, 0])
+        send(block, block, gather_send.at[h, 2], gather_recv.at[h, 2], pair)
     for h in range(2):
         for line, slot in ((row, 1), (1 - row, 2)):
             wait_arrival(
@@ -774,12 +788,12 @@
             routed, routed, vmem(2, capacity, width), routed, vmem(2, tokens, half),
             rows, rows, hidden, hidden, hidden, blocks, blocks, blocks, blocks,
             near, near, near, far, far, routed, pre, pre,
-            dma((len(operands),)), dma((2, experts)), dma((2, experts)), dma((2, 2)), dma((2, 2)),
+            dma((len(operands),)), dma((2, experts)), dma((2, experts)), dma((2, 2, 2)), dma((2, 2, 2)),
             dma((2, experts, 2)), dma((2, experts, 2)), dma((2, experts)), dma((2, experts)),
-            dma((2, experts, 4)), dma((2, experts, 4)), dma((2, 2)), dma((2, 2)),
+            dma((2, experts, 4)), dma((2, experts, 4)), dma((2, 2, 2)), dma((2, 2, 2)),
             dma((experts,)), dma((experts,)), dma((1,)), dma((1,)),
             dma((experts, 2)), dma((experts, 2)), dma((experts, 2)), dma((experts, 2)),
-            dma((experts, 2)), dma((experts, 2)), dma((experts,)), dma((experts,)),
+            dma((experts, 2)), dma((experts, 2)), dma((experts, 2)), dma((experts, 2)),
             dma((2, 3)), dma((2, 3)), dma((2, n_tp)), dma((2, n_tp)),
             dma((2,)), dma((2,)), dma((2, 3)), dma((2, 3)),
         ],
@@ -952,7 +966,7 @@
     n_tp = lax.axis_size("tp")
     halo = 16
     aligned = model_width % (seq_devices * 128) == 0
-    planned = aligned and experts == len(PLAN_CHUNKS) + 1 and n_tp == experts
+    planned = aligned and experts == len(PLAN_CHUNKS) + 1 == n_tp and capacity % 32 == 0
     if planned and top_count == 2 and conv_taps.shape[0] <= halo:
         operands = (
             routes.T, route_weights.T, moe_input, out_grad, gate_b, conv_out, gate_c, hidden_h,

time: 73 us -> 70 us (0.959)
  Pallas kernels: 71.7 us -> 69.1 us
    pallas_call x1, Pallas kernels: 69.2 us -> 66.5 us  [run_experts(): pl.pallas_call(functools.partial(expert_kernel, n_sp, n_tp), out_shape=(w...]
where the time goes in v5:
time: 70 us; the launch traced here: 69.9 us
  Pallas kernels  69.1 us (99%)
  between operations  0.81 us (1%)
    pallas_call x1, Pallas kernels, run_experts(): pl.pallas_call(functools.partial(expert_kernel, n_sp, n_tp), out_shape=(w...  66.5 us
    pallas_call x1, Pallas kernels, store(): pl.pallas_call(store_kernel, out_shape=tuple((jax.ShapeDtypeStruct(a.shap...  2.55 us

profile of v5, /device:TPU:0, one launch (start us, length us, event | category | flops | bytes accessed | tf_op | source)
XLA Modules:
  0.0 69.9 jit_solution(10672990469945790688)
XLA Ops:
  0.6 66.5 %shard_map.180 = (bf16[448,2048]{1,0:T(8,128)(2,1)S(1)}, bf16[448,2048]{1,0:T(8,128)(2,1)S(1)}, bf16[448,2048]{1,0:T(8,128)(2,1)S(1)}, f32[256,128]{1,0:T(8,128)...) custom-call(s32[2,128]{1,0:T(2,128)} %bitcast.8, ...), custom_call_target="tpu_custom_call" | custom-call | tf_op jit(solution)/shard_map/pallas_call | solution.py:777
  67.2 2.5 %shard_map.181 = (bf16[448,2048]{1,0:T(8,128)(2,1)}, bf16[448,2048]{1,0:T(8,128)(2,1)}, bf16[448,2048]{1,0:T(8,128)(2,1)}, f32[256,128]{1,0:T(8,128)}, bf16[128,...) custom-call(bf16[448,2048]{1,0:T(8,128)(2,1)S(1)} %get-tuple-element.21.refs_0_, ...), custom_call_target="tpu_custom_call" | custom-call | tf_op jit(solution)/shard_map/pallas_call | solution.py:818

commit v6 on v5

--- a/solution.py
+++ b/solution.py
@@ -659,12 +659,12 @@
     def block_columns(h, line, side_core):
         return columns(4 * h + 2 * side_core + line, half)
 
-    for j in PLAN_CHUNKS:
+    total = dot(chosen_ref[expert], out_back[expert], 0, 0)
+    for j in dict.fromkeys(stage[1] for stage in PLAN if stage[0] == "right" and stage[1]):
+        source = flipped(expert, j)
         for h in range(2):
-            block = out_back.at[flipped(expert, j), :, pl.ds(h * half, half)]
-            wait_arrival(block, back_recv.at[j, h])
-    one_hot = chosen_ref[...].reshape(experts * capacity, tokens)
-    total = dot(one_hot, out_back[...].reshape(experts * capacity, width), 0, 0)
+            wait_arrival(out_back.at[source, :, pl.ds(h * half, half)], back_recv.at[j, h])
+        total = total + dot(chosen_ref[source], out_back[source], 0, 0)
     guarded = []
     for h in range(2):
         cols = block_columns(h, row, core)

time: 70 us -> 70.1 us (level)
  no operation moved by 1% of the time
where the time goes in v6:
time: 70.1 us; the launch traced here: 69.9 us
  Pallas kernels  69.1 us (99%)
  between operations  0.81 us (1%)
    pallas_call x1, Pallas kernels, run_experts(): pl.pallas_call(functools.partial(expert_kernel, n_sp, n_tp), out_shape=(w...  66.6 us
    pallas_call x1, Pallas kernels, store(): pl.pallas_call(store_kernel, out_shape=tuple((jax.ShapeDtypeStruct(a.shap...  2.55 us

profile of v6, /device:TPU:0, one launch (start us, length us, event | category | flops | bytes accessed | tf_op | source)
XLA Modules:
  0.0 69.9 jit_solution(1453721222931777859)
XLA Ops:
  0.6 66.6 %shard_map.180 = (bf16[448,2048]{1,0:T(8,128)(2,1)S(1)}, bf16[448,2048]{1,0:T(8,128)(2,1)S(1)}, bf16[448,2048]{1,0:T(8,128)(2,1)S(1)}, f32[256,128]{1,0:T(8,128)...) custom-call(s32[2,128]{1,0:T(2,128)} %bitcast.8, ...), custom_call_target="tpu_custom_call" | custom-call | tf_op jit(solution)/shard_map/pallas_call | solution.py:777
  67.2 2.5 %shard_map.181 = (bf16[448,2048]{1,0:T(8,128)(2,1)}, bf16[448,2048]{1,0:T(8,128)(2,1)}, bf16[448,2048]{1,0:T(8,128)(2,1)}, f32[256,128]{1,0:T(8,128)}, bf16[128,...) custom-call(bf16[448,2048]{1,0:T(8,128)(2,1)S(1)} %get-tuple-element.21.refs_0_, ...), custom_call_target="tpu_custom_call" | custom-call | tf_op jit(solution)/shard_map/pallas_call | solution.py:818
